TPU v7x, 256 devices: a whole 4x4x8 slice. The times are simulated.
256 devices in a mesh: st: 64 (over z, y, core), tp: 4 (over x).
Axes of the slice: x: 4, y: 4, z: 8, core: 2. Of those that a mesh axis runs over, the one named last changes fastest.
Arguments:
- queries: bfloat16 [65536, 1024], P('st', 'tp'), may hold values from -540 to 540
- gate_pre: bfloat16 [65536, 1024], P('st', 'tp'), may hold values from -6 to 6
- cotangent: bfloat16 [65536, 1024], P('st', 'tp'), may hold values from -6 to 6
- store: bfloat16 [81920, 2048], P('st'), may hold values from -6 to 6
- store_gain: float32 [2048], replicated, may hold values from 0.1 to 1.9
- w_key: bfloat16 [2048, 1024], P(None, 'tp'), may hold values from -0.125 to 0.125
- w_value: bfloat16 [2048, 1024], P(None, 'tp'), may hold values from -0.125 to 0.125
- owners: int32 [512, 4], P('st'), may hold values from 0 to 63, all different within a row; in each aligned block of 8 rows (0 to 7, 8 to 15, ...) at most 1 rows name the same one
- slots: int32 [512, 4], P('st'), may hold values from 0 to 19
Outputs:
- grad_queries: float32 [65536, 1024], P('st', 'tp')
- grad_store: float32 [81920, 2048], P(('st', 'tp'))
- grad_w_value: float32 [2048, 1024], P('st', 'tp')
Inputs may be any that keep to these rules, and one draw needn't show every extreme that they name: Each block names 4 different owners. Among the blocks of one device no owner is named twice.
All inputs are finite; a program needn't handle non-finite values.
Results may differ from a plain program's by a relative error of at most 0.014.
Values may be sent and summed in bfloat16 or wider, within the bound.
A program may use at most 192 MiB of HBM per device.

v0:
```python
import functools

import jax
import jax.numpy as jnp
from jax import lax
from jax.experimental import pallas as pl
from jax.experimental.pallas import tpu as pltpu
from jax.sharding import PartitionSpec as P

HD = 128
PLEN = 64


EPS = 1e-06


def row_scale(store_rows):
    return lax.rsqrt(jnp.mean(store_rows * store_rows, axis=-1, keepdims=True) + EPS)


def contract(left, right):
    return lax.dot_general(
        left, right, (((1,), (1,)), ((), ())), preferred_element_type=jnp.float32
    )


def passage_plan(queries, gate_pre, cotangent, store, store_gain, w_key, w_value, owners, slots):
    st_size = lax.axis_size("st")
    tp_size = lax.axis_size("tp")
    blocks, per_block = owners.shape
    tok_rows, local_width = queries.shape
    head_dim = HD
    local_heads = local_width // head_dim
    block_len = tok_rows // blocks
    passage_len = PLEN
    rows_dev = store.shape[0]
    passages = rows_dev // passage_len
    slot_count = blocks * per_block
    slot_cap = (2 * slot_count + st_size - 1) // st_size
    store_rows = store.astype(jnp.float32)
    row_inverse = row_scale(store_rows)
    normed = (store_rows * row_inverse * store_gain).astype(jnp.bfloat16)
    key_table = jnp.dot(normed, w_key, preferred_element_type=jnp.float32).astype(jnp.bfloat16)
    value_table = jnp.dot(normed, w_value, preferred_element_type=jnp.float32).astype(jnp.bfloat16)
    key_table = key_table.reshape(passages, passage_len, local_width)
    value_table = value_table.reshape(passages, passage_len, local_width)
    owner_flat = owners.reshape(slot_count)
    slot_flat = slots.reshape(slot_count)
    slot_order = jnp.arange(slot_count, dtype=jnp.int32)
    earlier_same = (owner_flat[:, None] == owner_flat[None, :]) & (
        slot_order[None, :] < slot_order[:, None]
    )
    slot_rank = jnp.sum(earlier_same.astype(jnp.int32), axis=1)
    position = owner_flat * slot_cap + slot_rank
    places = jnp.arange(st_size * slot_cap, dtype=jnp.int32)
    slot_hits = position[:, None] == places[None, :]
    requests = jnp.sum(jnp.where(slot_hits, slot_flat[:, None], 0), axis=0)
    requests = requests.reshape(st_size, slot_cap)
    asked_ids = lax.all_to_all(requests, "st", split_axis=0, concat_axis=0, tiled=True)
    asked_flat = asked_ids.reshape(-1)
    shape_out = asked_ids.shape + (passage_len, local_width)
    picked_keys = jnp.take(key_table, asked_flat, axis=0).reshape(shape_out)
    picked_values = jnp.take(value_table, asked_flat, axis=0).reshape(shape_out)
    sent_keys = lax.all_to_all(picked_keys, "st", split_axis=0, concat_axis=0, tiled=True)
    sent_values = lax.all_to_all(picked_values, "st", split_axis=0, concat_axis=0, tiled=True)
    got_keys, got_values, asked_ids = (sent_keys, sent_values, asked_ids)
    span = per_block * passage_len
    mine_keys = jnp.take(
        got_keys.reshape(st_size * slot_cap, passage_len, local_width), position, axis=0
    )
    mine_values = jnp.take(
        got_values.reshape(st_size * slot_cap, passage_len, local_width), position, axis=0
    )
    mine_keys = mine_keys.reshape(blocks, span, local_heads, head_dim)
    mine_values = mine_values.reshape(blocks, span, local_heads, head_dim)
    score_scale = head_dim ** (-0.5)
    query_blocks = queries.reshape(blocks, block_len, local_heads, head_dim)
    gate_open = jax.nn.sigmoid(gate_pre.astype(jnp.float32))
    grad_in = (gate_open * cotangent.astype(jnp.float32)).astype(jnp.bfloat16)
    grad_in = grad_in.reshape(blocks, block_len, local_heads, head_dim)
    scores = (
        jnp.einsum("bqhd,bkhd->bhqk", query_blocks, mine_keys, preferred_element_type=jnp.float32)
        * score_scale
    )
    shifted = scores - jnp.max(scores, axis=-1, keepdims=True)
    weights = jnp.exp(shifted)
    weights = weights / jnp.sum(weights, axis=-1, keepdims=True)
    weights_half = weights.astype(jnp.bfloat16)
    attended = jnp.einsum(
        "bhqk,bkhd->bqhd", weights_half, mine_values, preferred_element_type=jnp.float32
    )
    row_delta = jnp.sum(grad_in.astype(jnp.float32) * attended, axis=-1)
    grad_weights = jnp.einsum(
        "bqhd,bkhd->bhqk", grad_in, mine_values, preferred_element_type=jnp.float32
    )
    grad_scores = weights * (grad_weights - jnp.transpose(row_delta, (0, 2, 1))[..., None])
    grad_half = grad_scores.astype(jnp.bfloat16)
    grad_queries = (
        jnp.einsum("bhqk,bkhd->bqhd", grad_half, mine_keys, preferred_element_type=jnp.float32)
        * score_scale
    )
    grad_queries = grad_queries.reshape(tok_rows, local_width)
    grad_keys = (
        jnp.einsum("bhqk,bqhd->bkhd", grad_half, query_blocks, preferred_element_type=jnp.float32)
        * score_scale
    )
    grad_values = jnp.einsum(
        "bhqk,bqhd->bkhd", weights_half, grad_in, preferred_element_type=jnp.float32
    )
    grad_keys = grad_keys.reshape(slot_count, passage_len, local_width)
    grad_values = grad_values.reshape(slot_count, passage_len, local_width)
    empty_slots = jnp.zeros((st_size * slot_cap, passage_len, local_width), jnp.bfloat16)
    outgoing_keys = empty_slots.at[position].set(grad_keys.astype(jnp.bfloat16))
    outgoing_values = empty_slots.at[position].set(grad_values.astype(jnp.bfloat16))
    back_keys, back_values = (
        lax.all_to_all(outgoing_keys, "st", split_axis=0, concat_axis=0, tiled=True),
        lax.all_to_all(outgoing_values, "st", split_axis=0, concat_axis=0, tiled=True),
    )
    asked_flat = asked_ids.reshape(-1)
    owner_pick = (asked_flat[None, :] == jnp.arange(passages, dtype=jnp.int32)[:, None]).astype(
        jnp.bfloat16
    )
    passage_keys = jnp.dot(
        owner_pick,
        back_keys.reshape(st_size * slot_cap, passage_len * local_width),
        preferred_element_type=jnp.float32,
    )
    passage_values = jnp.dot(
        owner_pick,
        back_values.reshape(st_size * slot_cap, passage_len * local_width),
        preferred_element_type=jnp.float32,
    )
    passage_keys = passage_keys.astype(jnp.bfloat16).reshape(rows_dev, local_width)
    passage_values = passage_values.astype(jnp.bfloat16).reshape(rows_dev, local_width)
    weight_terms = lax.dot_general(
        normed, passage_values, (((0,), (0,)), ((), ())), preferred_element_type=jnp.float32
    )
    grad_w_value = lax.psum_scatter(weight_terms, "st", scatter_dimension=0, tiled=True)
    quarter = rows_dev // tp_size
    whole_key, whole_value = (
        lax.all_gather(w_key, "tp", axis=1, tiled=True),
        lax.all_gather(w_value, "tp", axis=1, tiled=True),
    )
    own_keys, own_values = (
        lax.all_to_all(passage_keys, "tp", split_axis=0, concat_axis=1, tiled=True),
        lax.all_to_all(passage_values, "tp", split_axis=0, concat_axis=1, tiled=True),
    )
    grad_normed = contract(own_keys, whole_key) + contract(own_values, whole_value)
    first_row = lax.axis_index("tp") * quarter
    own_rows = lax.dynamic_slice_in_dim(store_rows, first_row, quarter, 0)
    own_inverse = lax.dynamic_slice_in_dim(row_inverse, first_row, quarter, 0)
    unit_rows = own_rows * own_inverse
    grad_unit = grad_normed * store_gain
    grad_store = own_inverse * (
        grad_unit - unit_rows * jnp.mean(grad_unit * unit_rows, axis=-1, keepdims=True)
    )
    return (grad_queries, grad_store, grad_w_value)


FAR = -1e30
MESH = pl.DeviceIdType.MESH


def place_of(index, n):
    odd = index % 2
    return (1 - odd) * (index // 2) + odd * (n - 1 - index // 2)


def index_at(place, n):
    place = (place + 2 * n) % n
    back = place // (n // 2)
    return (1 - back) * (2 * place) + back * (2 * (n - 1 - place) + 1)


def greet(others):
    barrier = pltpu.get_barrier_semaphore()
    for axis, other in others:
        pl.semaphore_signal(barrier, inc=1, device_id={axis: other}, device_id_type=MESH)
    pl.semaphore_wait(barrier, len(others))


def gather_kernel(n, q_ref, g_ref, i_ref, x_ref, gain_ref, wk_ref, wv_ref, q_all, g_all, i_all, normed_ref, kt_ref, vt_ref, send_sem, recv_sem, own_sem):
    me = lax.axis_index("st")
    place = place_of(me, n)
    right, left = index_at(place + 1, n), index_at(place - 1, n)
    half_rows = q_ref.shape[0] // 2
    pairs = ((q_ref, q_all), (g_ref, g_all), (i_ref, i_all))
    greet((("st", left), ("st", right)))
    own = []
    for number, (src, dst) in enumerate(pairs):
        copy = pltpu.make_async_copy(src, dst.at[me], own_sem.at[number])
        copy.start()
        own.append(copy)
    hops = n // 2
    parts = ((2, 0), (0, 0), (0, 1), (1, 0), (1, 1))

    def last_on(side, part):
        return parts[part][1] == side

    def piece(side, step, part):
        number, half = parts[part]
        src, dst = pairs[number]
        origin = index_at(place - step, n) if side == 0 else index_at(place + step, n)
        rows = pl.ds(0, i_ref.shape[0]) if number == 2 else pl.ds(half * half_rows, half_rows)
        return pltpu.make_async_remote_copy(
            src_ref=src.at[rows] if step == 0 else dst.at[origin, rows],
            dst_ref=dst.at[origin, rows],
            send_sem=send_sem.at[side, step, part],
            recv_sem=recv_sem.at[side, step, part],
            device_id={"st": right if side == 0 else left},
            device_id_type=MESH,
        )

    count = x_ref.shape[0] // 128

    def project(chunk):
        rows = pl.ds(chunk * 128, 128)
        wide = x_ref[rows].astype(jnp.float32)
        normed = (wide * row_scale(wide) * gain_ref[...]).astype(jnp.bfloat16)
        normed_ref[rows] = normed
        kt_ref[rows] = jnp.dot(normed, wk_ref[...], preferred_element_type=jnp.float32).astype(jnp.bfloat16)
        vt_ref[rows] = jnp.dot(normed, wv_ref[...], preferred_element_type=jnp.float32).astype(jnp.bfloat16)

    chunk = 0
    started = []
    for step in range(hops):
        for part in range(5):
            for side in range(2):
                if step < hops - 1 or last_on(side, part):
                    if step > 0:
                        piece(side, step - 1, part).wait_recv()
                    copy = piece(side, step, part)
                    copy.start()
                    started.append(copy)
            if part > 0 and chunk < count:
                project(chunk)
                chunk += 1
    for rest in range(chunk, count):
        project(rest)
    for part in range(5):
        for side in range(2):
            if not last_on(side, part):
                piece(side, hops - 2, part).wait_recv()
    for part in range(5):
        piece(parts[part][1], hops - 1, part).wait_recv()
    for copy in own:
        copy.wait()
    for copy in started:
        copy.wait_send()


def ring_gather(queries, grad_in, named, store, gain, w_key, w_value, n):
    hops = n // 2
    vmem = pl.BlockSpec(memory_space=pltpu.VMEM)
    sources = (queries, grad_in, named)
    return pl.pallas_call(
        functools.partial(gather_kernel, n),
        out_shape=tuple(jax.ShapeDtypeStruct((n,) + x.shape, x.dtype) for x in sources)
        + (jax.ShapeDtypeStruct(store.shape, jnp.bfloat16),)
        + (jax.ShapeDtypeStruct((store.shape[0], w_key.shape[1]), jnp.bfloat16),) * 2,
        in_specs=[vmem] * 7,
        out_specs=(vmem,) * 6,
        scratch_shapes=[
            pltpu.SemaphoreType.DMA((2, hops, 5)),
            pltpu.SemaphoreType.DMA((2, hops, 5)),
            pltpu.SemaphoreType.DMA((3,)),
        ],
        cost_estimate=pl.CostEstimate(flops=10**10, bytes_accessed=10**7, transcendentals=0),
        compiler_params=pltpu.CompilerParams(collective_id=0, has_side_effects=True, vmem_limit_bytes=40 << 20),
        name="ring_gather",
    )(*sources, store, gain[None], w_key, w_value)


def join_kernel(n, heads, x_ref, out_ref, got, mine, send_sem, recv_sem, own_sem):
    me = lax.axis_index("st")
    peers = [(me + away) % n for away in range(1, n)]
    greet([("st", peer) for peer in peers])

    def piece(phase, away):
        peer = (me + away) % n
        return pltpu.make_async_remote_copy(
            src_ref=x_ref.at[peer] if phase == 0 else mine,
            dst_ref=got.at[me] if phase == 0 else out_ref.at[me],
            send_sem=send_sem.at[phase, away],
            recv_sem=recv_sem.at[phase, away],
            device_id={"st": peer},
            device_id_type=MESH,
        )

    for away in range(1, n):
        piece(0, away).start()
    local = pltpu.make_async_copy(x_ref.at[me], got.at[me], own_sem.at[0])
    local.start()
    local.wait()
    for away in range(1, n):
        piece(0, away).wait()
    for head in range(heads):
        logs = [got[owner, :, 2 * head] for owner in range(n)]
        top = functools.reduce(jnp.maximum, logs)
        shares = [jnp.exp(one - top) for one in logs]
        total = sum(shares)
        mine[:, 2 * head] = top + jnp.log(total)
        mine[:, 2 * head + 1] = sum(share * got[owner, :, 2 * head + 1] for owner, share in enumerate(shares)) / total
    out_ref[me] = mine[...]
    for away in range(1, n):
        piece(1, away).start()
    for away in range(1, n):
        piece(1, away).wait()


def join_stats(stats, n):
    total, rows, width = stats.shape
    blocks = total // n
    vmem = pl.BlockSpec(memory_space=pltpu.VMEM)
    joined = pl.pallas_call(
        functools.partial(join_kernel, n, rows // 2),
        out_shape=jax.ShapeDtypeStruct((n, blocks, rows, width), jnp.float32),
        in_specs=[vmem],
        out_specs=vmem,
        scratch_shapes=[
            pltpu.VMEM((n, blocks, rows, width), jnp.float32),
            pltpu.VMEM((blocks, rows, width), jnp.float32),
            pltpu.SemaphoreType.DMA((2, n)),
            pltpu.SemaphoreType.DMA((2, n)),
            pltpu.SemaphoreType.DMA((1,)),
        ],
        cost_estimate=pl.CostEstimate(flops=10**9, bytes_accessed=10**6, transcendentals=0),
        compiler_params=pltpu.CompilerParams(collective_id=2, has_side_effects=True),
        name="join_stats",
    )(stats.reshape(n, blocks, rows, width))
    return joined.reshape(total, rows, width)


def scatter_kernel(n, tp, parts, x_ref, w_ref, k_ref, v_ref, out_ref, gw_ref, ok_ref, ov_ref, send_buf, recv_buf, send_sem, recv_sem, tp_send, tp_recv, own_sem):
    me = lax.axis_index("st")
    mine = lax.axis_index("tp")
    place = place_of(me, n)
    right, left = index_at(place + 1, n), index_at(place - 1, n)
    tokens = x_ref.shape[1]
    greet([("st", left), ("st", right)] + [("tp", (mine + away) % tp) for away in range(1, tp)])
    quarter, width = ok_ref.shape[0], k_ref.shape[1]
    columns = pl.ds(pl.multiple_of(mine * width, 128), width)

    def across(number, away):
        src, dst = ((k_ref, ok_ref), (v_ref, ov_ref))[number]
        peer = (mine + away) % tp
        return pltpu.make_async_remote_copy(
            src_ref=src.at[pl.ds(pl.multiple_of(peer * quarter, 16), quarter)],
            dst_ref=dst.at[:, columns],
            send_sem=tp_send.at[number, away],
            recv_sem=tp_recv.at[number, away],
            device_id={"tp": peer},
            device_id_type=MESH,
        )

    def kept(number):
        src, dst = ((k_ref, ok_ref), (v_ref, ov_ref))[number]
        return pltpu.make_async_copy(
            src.at[pl.ds(pl.multiple_of(mine * quarter, 16), quarter)], dst.at[:, columns], own_sem.at[number]
        )

    for number in range(2):
        kept(number).start()
        for away in range(1, tp):
            across(number, away).start()
    hops = n // 2

    def used(side, step, part):
        return step > 0 or parts[part][3] == side

    def piece(side, step, part):
        number, first, count, _ = parts[part]
        at = pl.ds(number * tokens + first, count)
        return pltpu.make_async_remote_copy(
            src_ref=send_buf.at[side, step, at],
            dst_ref=recv_buf.at[side, step, at],
            send_sem=send_sem.at[side, step, part],
            recv_sem=recv_sem.at[side, step, part],
            device_id={"st": right if side == 0 else left},
            device_id_type=MESH,
        )

    started = []
    for step in range(hops):
        for part, (number, first, count, _) in enumerate(parts):
            for side in range(2):
                if not used(side, step, part):
                    continue
                distance = hops - step
                dest = index_at(place + distance, n) if side == 0 else index_at(place - distance, n)
                at = pl.ds(number * tokens + first, count)
                total = (x_ref, w_ref)[number][dest, pl.ds(first, count)]
                if step > 0 and used(side, step - 1, part):
                    piece(side, step - 1, part).wait_recv()
                    total = (total.astype(jnp.float32) + recv_buf[side, step - 1, at].astype(jnp.float32)).astype(jnp.bfloat16)
                send_buf[side, step, at] = total
                copy = piece(side, step, part)
                copy.start()
                started.append(copy)
    for part, (number, first, count, _) in enumerate(parts):
        at = pl.ds(number * tokens + first, count)
        total = (x_ref, w_ref)[number][me, pl.ds(first, count)].astype(jnp.float32)
        for side in range(2):
            piece(side, hops - 1, part).wait_recv()
            total = total + recv_buf[side, hops - 1, at].astype(jnp.float32)
        (out_ref, gw_ref)[number][pl.ds(first, count)] = total
    for number in range(2):
        kept(number).wait()
        for away in range(1, tp):
            across(number, away).wait()
    for copy in started:
        copy.wait_send()


def ring_scatter(terms, weight_terms, keys, values, n, tp):
    rows, width = terms.shape[1:]
    rest = weight_terms.shape[1]
    hops = n // 2
    parts = ((0, 0, rows // 4, 0), (0, rows // 2, rows // 4, 1), (0, rows // 4, rows // 4, 0),
             (0, 3 * rows // 4, rows // 4, 1), (1, 0, rest // 2, 0), (1, rest // 2, rest // 2, 1))
    vmem = pl.BlockSpec(memory_space=pltpu.VMEM)
    own = jax.ShapeDtypeStruct((keys.shape[0] // tp, width * tp), jnp.bfloat16)
    return pl.pallas_call(
        functools.partial(scatter_kernel, n, tp, parts),
        out_shape=(
            jax.ShapeDtypeStruct((rows, width), jnp.float32),
            jax.ShapeDtypeStruct((rest, width), jnp.float32),
            own,
            own,
        ),
        in_specs=[vmem] * 4,
        out_specs=(vmem,) * 4,
        scratch_shapes=[
            pltpu.VMEM((2, hops, rows + rest, width), jnp.bfloat16),
            pltpu.VMEM((2, hops, rows + rest, width), jnp.bfloat16),
            pltpu.SemaphoreType.DMA((2, hops, len(parts))),
            pltpu.SemaphoreType.DMA((2, hops, len(parts))),
            pltpu.SemaphoreType.DMA((2, tp)),
            pltpu.SemaphoreType.DMA((2, tp)),
            pltpu.SemaphoreType.DMA((2,)),
        ],
        cost_estimate=pl.CostEstimate(flops=5 * 10**9, bytes_accessed=10**7, transcendentals=0),
        compiler_params=pltpu.CompilerParams(collective_id=1, has_side_effects=True, vmem_limit_bytes=50 << 20),
        name="ring_scatter",
    )(terms, weight_terms, keys, values)


NT = (((1,), (1,)), ((), ()))
TN = (((0,), (0,)), ((), ()))


def dot(left, right, dims=(((1,), (0,)), ((), ()))):
    return lax.dot_general(left, right, dims, preferred_element_type=jnp.float32)


def items_of(table, total, heads, turn):
    items = []
    for lane in range(2):
        block = table[total + 2 * turn + lane]
        picked = table[block]
        for head in range(heads):
            items.append((block, picked >= 0, jnp.maximum(picked, 0), head, pl.ds(head * HD, HD)))
    return items


def raw_products(items, q_ref, g_ref, k_ref, v_ref):
    scale = HD ** (-0.5)
    scores = [dot(k_ref[picked, :, cols], q_ref[block, :, cols], NT) * scale for block, _, picked, _, cols in items]
    grads = [dot(v_ref[picked, :, cols], g_ref[block, :, cols], NT) for block, _, picked, _, cols in items]
    return scores, grads


def stats_kernel(heads, table, q_ref, g_ref, k_ref, v_ref, out_ref):
    total, _, block_len = out_ref.shape

    @pl.loop(0, total)
    def _(block):
        for head in range(heads):
            out_ref[block, 2 * head] = jnp.full((block_len,), FAR, jnp.float32)
            out_ref[block, 2 * head + 1] = jnp.zeros((block_len,), jnp.float32)

    @pl.loop(0, (table[2 * total] + 1) // 2)
    def _(turn):
        items = items_of(table, total, heads, turn)
        scores, grads = raw_products(items, q_ref, g_ref, k_ref, v_ref)
        tops = [jnp.max(one, axis=0, keepdims=True) for one in scores]
        raised = [jnp.exp(one - top) for one, top in zip(scores, tops)]
        totals = [jnp.sum(one, axis=0, keepdims=True) for one in raised]
        means = [jnp.sum(one * two, axis=0, keepdims=True) / three for one, two, three in zip(raised, grads, totals)]
        logs = [top + jnp.log(one) for top, one in zip(tops, totals)]
        for number, (block, live, _, head, _) in enumerate(items):
            @pl.when(live)
            def _():
                out_ref[block, pl.ds(2 * head, 1)] = logs[number]
                out_ref[block, pl.ds(2 * head + 1, 1)] = means[number]


def grads_kernel(heads, table, q_ref, g_ref, k_ref, v_ref, s_ref, dq_ref, pk_ref, pv_ref, dk_acc, dv_acc):
    scale = HD ** (-0.5)
    total = dq_ref.shape[0]
    dk_acc[...] = jnp.zeros_like(dk_acc)
    dv_acc[...] = jnp.zeros_like(dv_acc)

    @pl.loop(table[2 * total], total)
    def _(at):
        dq_ref[table[total + at]] = jnp.zeros(dq_ref.shape[1:], jnp.bfloat16)

    @pl.loop(0, (table[2 * total] + 1) // 2)
    def _(turn):
        items = items_of(table, total, heads, turn)
        scores, grads = raw_products(items, q_ref, g_ref, k_ref, v_ref)
        weights, halves = [], []
        for (block, _, _, head, _), score, grad in zip(items, scores, grads):
            weight = jnp.exp(score - s_ref[block, pl.ds(2 * head, 1)])
            halves.append((weight * (grad - s_ref[block, pl.ds(2 * head + 1, 1)])).astype(jnp.bfloat16))
            weights.append(weight.astype(jnp.bfloat16))
        steps, keys, values = [], [], []
        for (block, _, picked, _, cols), weight, half in zip(items, weights, halves):
            keys.append(dot(half, q_ref[block, :, cols]) * scale)
            values.append(dot(weight, g_ref[block, :, cols]))
            steps.append((dot(half, k_ref[picked, :, cols], TN) * scale).astype(jnp.bfloat16))
        for number, (block, live, picked, _, cols) in enumerate(items):
            @pl.when(live)
            def _():
                dq_ref[block, :, cols] = steps[number]
                dk_acc[picked, :, cols] += keys[number]
                dv_acc[picked, :, cols] += values[number]

    pk_ref[...] = dk_acc[...].astype(jnp.bfloat16)
    pv_ref[...] = dv_acc[...].astype(jnp.bfloat16)


def table_of(ids):
    total = ids.shape[0]
    spot = jnp.arange(total, dtype=jnp.int32)
    idle = (ids < 0).astype(jnp.int32)
    sort_key = idle * total + spot
    rank = jnp.sum((sort_key[None, :] < sort_key[:, None]).astype(jnp.int32), axis=1)
    order = jnp.sum(jnp.where(rank[None, :] == spot[:, None], spot[None, :], 0), axis=1)
    count = total - jnp.sum(idle)
    return jnp.concatenate([ids, order, count[None]])


def query_plan(queries, gate_pre, cotangent, store, store_gain, w_key, w_value, owners, slots):
    n = lax.axis_size("st")
    tp_size = lax.axis_size("tp")
    me = lax.axis_index("st")
    blocks, per_block = owners.shape
    tok_rows, local_width = queries.shape
    heads = local_width // HD
    block_len = tok_rows // blocks
    rows_dev = store.shape[0]
    passages = rows_dev // PLEN
    named = jnp.pad(owners * passages + slots, ((0, 0), (0, 128 - per_block)), constant_values=-1)
    gate_open = jax.nn.sigmoid(gate_pre.astype(jnp.float32))
    grad_in = (gate_open * cotangent.astype(jnp.float32)).astype(jnp.bfloat16)
    q_all, g_all, all_named, normed, key_table, value_table = ring_gather(
        queries, grad_in, named, store, store_gain, w_key, w_value, n
    )
    held = all_named.reshape(n * blocks, 128)[:, :per_block] - me * passages
    ids = jnp.max(jnp.where((held >= 0) & (held < passages), held, -1), axis=1)
    key_table = key_table.reshape(passages, PLEN, local_width)
    value_table = value_table.reshape(passages, PLEN, local_width)
    table = table_of(ids)
    total = n * blocks
    q_blocks = q_all.reshape(total, block_len, local_width)
    g_blocks = g_all.reshape(total, block_len, local_width)
    smem = pl.BlockSpec(memory_space=pltpu.SMEM)
    vmem = pl.BlockSpec(memory_space=pltpu.VMEM)
    stats = pl.pallas_call(
        functools.partial(stats_kernel, heads),
        out_shape=jax.ShapeDtypeStruct((total, 2 * heads, block_len), jnp.float32),
        in_specs=[smem] + [vmem] * 4,
        out_specs=vmem,
        compiler_params=pltpu.CompilerParams(vmem_limit_bytes=40 << 20),
        name="stats",
    )(table, q_blocks, g_blocks, key_table, value_table)
    joined = join_stats(stats, n)
    dq, passage_keys, passage_values = pl.pallas_call(
        functools.partial(grads_kernel, heads),
        out_shape=(
            jax.ShapeDtypeStruct((total, block_len, local_width), jnp.bfloat16),
            jax.ShapeDtypeStruct((passages, PLEN, local_width), jnp.bfloat16),
            jax.ShapeDtypeStruct((passages, PLEN, local_width), jnp.bfloat16),
        ),
        in_specs=[smem] + [vmem] * 5,
        out_specs=(vmem,) * 3,
        scratch_shapes=[pltpu.VMEM((passages, PLEN, local_width), jnp.float32)] * 2,
        compiler_params=pltpu.CompilerParams(vmem_limit_bytes=40 << 20),
        name="grads",
    )(table, q_blocks, g_blocks, key_table, value_table, joined)
    dq = dq.reshape(n, tok_rows, local_width)
    passage_keys = passage_keys.reshape(rows_dev, local_width)
    passage_values = passage_values.reshape(rows_dev, local_width)
    weight_terms = lax.dot_general(
        normed, passage_values, (((0,), (0,)), ((), ())), preferred_element_type=jnp.float32
    ).astype(jnp.bfloat16)
    whole_key, whole_value = (
        lax.all_gather(w_key, "tp", axis=1, tiled=True),
        lax.all_gather(w_value, "tp", axis=1, tiled=True),
    )
    quarter = rows_dev // tp_size
    grad_queries, grad_w_value, own_keys, own_values = ring_scatter(
        dq, weight_terms.reshape(n, -1, local_width), passage_keys, passage_values, n, tp_size
    )
    grad_normed = contract(own_keys, whole_key) + contract(own_values, whole_value)
    first_row = lax.axis_index("tp") * quarter
    own_rows = lax.dynamic_slice_in_dim(store, first_row, quarter, 0).astype(jnp.float32)
    own_inverse = row_scale(own_rows)
    unit_rows = own_rows * own_inverse
    grad_unit = grad_normed * store_gain
    grad_store = own_inverse * (
        grad_unit - unit_rows * jnp.mean(grad_unit * unit_rows, axis=-1, keepdims=True)
    )
    return (grad_queries, grad_store, grad_w_value)


def local(*arrays):
    queries, owners = arrays[0], arrays[7]
    n = lax.axis_size("st")
    slot_cap = (2 * owners.size + n - 1) // n
    if n % 2 == 0 and n >= 4 and 8 * slot_cap * PLEN >= 3 * queries.shape[0]:
        return query_plan(*arrays)
    return passage_plan(*arrays)


def solution(mesh):
    placed = (
        P("st", "tp"),
        P("st", "tp"),
        P("st", "tp"),
        P("st", None),
        P(),
        P(None, "tp"),
        P(None, "tp"),
        P("st", None),
        P("st", None),
    )
    return jax.shard_map(
        local,
        mesh=mesh,
        in_specs=placed,
        out_specs=(P("st", "tp"), P(("st", "tp"), None), P("st", "tp")),
        check_vma=False,
    )
```

profile of v0, /device:TPU:1, one launch (start us, length us, event | category | flops | bytes accessed | tf_op | source)
XLA Modules:
  0.0 391.0 jit_solution(2666753423177931793)
XLA Ops:
  9.0 0.8 copy.96
  10.7 13.1 %all-to-all-start = ((s32[64,1,1]{2,1,0:T(1,128)}), s32[64,1,1]{2,1,0:T(1,128)S(1)}, u32[]{:S(2)}, u32[]{:S(2)}) async-start(s32[64,1,1]{2,1,0:T(1,128)} %copy.97), calls=%async_computation | async-start | bytes 65536 | tf_op jit(solution)/shard_map/all_to_all | solution.py:59
  23.9 3.7 multiply_reduce_fusion
  27.9 3.0 convolution_convert_fusion.2
  30.9 1.7 convolution_convert_fusion.3
  33.2 1.2 reduce
  35.1 2.0 gather_fusion.2
  37.1 3.3 select_bitcast_fusion
  40.5 59.4 %all_to_all.67 = bf16[64,1,64,256]{3,2,1,0:T(8,128)(2,1)} all-to-all(bf16[64,1,64,256]{3,2,1,0:T(8,128)(2,1)S(1)} %get-tuple-element.21), channel_id=1, replica_groups=mesh['st'=64,'tp'=4] {'st'}, dimensions={0} | all-to-all | bytes 4194304 | tf_op jit(solution)/shard_map/all_to_all | solution.py:65
  99.9 7.3 %all-to-all-start.1 = ((bf16[64,1,64,256]{3,2,1,0:T(8,128)(2,1)}), bf16[64,1,64,256]{3,2,1,0:T(8,128)(2,1)}, u32[]{:S(2)}, u32[]{:S(2)}) async-start(bf16[64,1,64,256]{3,2,1,0:T(8,128)(2,1)} %get-tuple-element.22), calls=%async_computation.1 | async-start | bytes 4194304 | tf_op jit(solution)/shard_map/all_to_all | solution.py:64
  109.3 2.4 gather_fusion.3
  111.7 45.1 %all-to-all-done.1 = bf16[64,1,64,256]{3,2,1,0:T(8,128)(2,1)} async-done(((bf16[64,1,64,256]{3,2,1,0:T(8,128)(2,1)}), bf16[64,1,64,256]{3,2,1,0:T(8,128)(2,1)}, u32[]{:S(2)}, u32[]{:S(2)}) %all-to-all-start.1) | async-done | bytes 2097184 | tf_op jit(solution)/shard_map/all_to_all | solution.py:64
  156.8 2.2 gather_fusion.1
  159.0 1.6 broadcast_select_fusion
  160.6 1.3 reshape.153
  163.1 1.6 fusion.25
  164.8 1.3 copy-done.7
  166.6 0.8 copy.116
  168.1 1.6 broadcast_in_dim.52.clone.1
  169.7 4.7 %scatter_fusion.1 = bf16[64,64,256]{2,1,0:T(8,128)(2,1)} fusion(bf16[64,64,256]{2,1,0:T(8,128)(2,1)} %broadcast_in_dim.52.clone.1, s32[32]{0:T(128)S(1)} %fusion.20, bf16[32,64,256]{2,1,0:T(8,128)(2,1)S(1)} %reshape.209), kind=kCustom, calls=%fused_computation.5 | custom fusion | bytes 3145856 | tf_op jit(solution)/shard_map/scatter | solution.py:114
  174.4 6.9 %all-to-all-start.5 = ((bf16[64,64,256]{2,1,0:T(8,128)(2,1)}), bf16[64,64,256]{2,1,0:T(8,128)(2,1)S(1)}, u32[]{:S(2)}, u32[]{:S(2)}) async-start(bf16[64,64,256]{2,1,0:T(8,128)(2,1)} %scatter_fusion.1), calls=%async_computation.5 | async-start | bytes 4194304 | tf_op jit(solution)/shard_map/all_to_all | solution.py:117
  182.1 2.1 reshape.159
  184.2 3.6 copy.104
  187.8 2.6 fusion.11
  191.5 1.0 copy-done.3
  192.9 2.0 copy.112
  195.0 2.5 reshape.201
  197.5 1.6 broadcast_in_dim.52.clone
  199.1 5.3 %scatter_fusion = bf16[64,64,256]{2,1,0:T(8,128)(2,1)} fusion(bf16[64,64,256]{2,1,0:T(8,128)(2,1)} %broadcast_in_dim.52.clone, s32[32]{0:T(128)S(1)} %fusion.20, bf16[32,64,256]{2,1,0:T(8,128)(2,1)} %reshape.201), kind=kCustom, calls=%fused_computation.4 | custom fusion | bytes 3145856 | tf_op jit(solution)/shard_map/scatter | solution.py:113
  204.4 26.7 %all-to-all-done.5 = bf16[64,64,256]{2,1,0:T(8,128)(2,1)S(1)} async-done(((bf16[64,64,256]{2,1,0:T(8,128)(2,1)}), bf16[64,64,256]{2,1,0:T(8,128)(2,1)S(1)}, u32[]{:S(2)}, u32[]{:S(2)}) %all-to-all-start.5) | async-done | bytes 2097184 | tf_op jit(solution)/shard_map/all_to_all | solution.py:117
  231.0 7.2 %all-to-all-start.3 = ((bf16[64,64,256]{2,1,0:T(8,128)(2,1)}), bf16[64,64,256]{2,1,0:T(8,128)(2,1)}, u32[]{:S(2)}, u32[]{:S(2)}) async-start(bf16[64,64,256]{2,1,0:T(8,128)(2,1)} %scatter_fusion), calls=%async_computation.3 | async-start | bytes 4194304 | tf_op jit(solution)/shard_map/all_to_all | solution.py:116
  238.5 1.3 copy.133
  240.6 5.8 %fusion.24 = f32[2048,256]{1,0:T(8,128)} fusion(bf16[1280,256]{1,0:T(8,128)(2,1)S(1)} %reshape.164, f32[2048]{0:T(1024)S(1)} %copy-done.16, f32[1280]{0:T(1024)S(1)} %add_rsqrt_fusion, bf16[1280,2048]{1,0:T(8,128)(2,1)} %param.16), kind=kOutput, calls=%fused_computation.65 | convolution fusion | flops 1352663040 | bytes 8008704 | tf_op jit(solution)/shard_map/dot_general | solution.py:135
  246.5 41.4 %all-to-all-done.3 = bf16[64,64,256]{2,1,0:T(8,128)(2,1)} async-done(((bf16[64,64,256]{2,1,0:T(8,128)(2,1)}), bf16[64,64,256]{2,1,0:T(8,128)(2,1)}, u32[]{:S(2)}, u32[]{:S(2)}) %all-to-all-start.3) | async-done | bytes 2097184 | tf_op jit(solution)/shard_map/all_to_all | solution.py:116
  287.8 2.9 copy.132
  291.1 1.3 all_to_all.51
  292.4 4.0 %all-to-all-start.4 = ((bf16[4,320,256]{2,1,0:T(8,128)(2,1)}), bf16[4,320,256]{2,1,0:T(8,128)(2,1)S(1)}, u32[]{:S(2)}, u32[]{:S(2)}) async-start(bf16[4,320,256]{2,1,0:T(8,128)(2,1)} %all_to_all.51), calls=%async_computation.4 | async-start | bytes 1310720 | tf_op jit(solution)/shard_map/all_to_all | solution.py:145
  296.4 1.3 all_to_all.56
  297.7 7.0 %all-to-all-done.4 = bf16[4,320,256]{2,1,0:T(8,128)(2,1)S(1)} async-done(((bf16[4,320,256]{2,1,0:T(8,128)(2,1)}), bf16[4,320,256]{2,1,0:T(8,128)(2,1)S(1)}, u32[]{:S(2)}, u32[]{:S(2)}) %all-to-all-start.4) | async-done | bytes 655392 | tf_op jit(solution)/shard_map/all_to_all | solution.py:145
  304.7 4.4 %all-to-all-start.6 = ((bf16[4,320,256]{2,1,0:T(8,128)(2,1)}), bf16[4,320,256]{2,1,0:T(8,128)(2,1)}, u32[]{:S(2)}, u32[]{:S(2)}) async-start(bf16[4,320,256]{2,1,0:T(8,128)(2,1)} %all_to_all.56), calls=%async_computation.6 | async-start | bytes 1310720 | tf_op jit(solution)/shard_map/all_to_all | solution.py:146
  309.2 8.0 %convert_element_type.58 = f32[1280,2048]{1,0:T(8,128)} convert(bf16[1280,2048]{1,0:T(8,128)(2,1)} %param.16) | non-fusion elementwise | flops 2621440 | bytes 15728640 | tf_op jit(solution)/shard_map/convert_element_type | solution.py:40
  318.4 1.0 copy.139
  319.4 0.9 copy.129
  320.3 1.2 copy.130
  321.5 4.0 %fusion.26 = f32[320,2048]{1,0:T(8,128)S(1)} fusion(bf16[320,1024]{1,0:T(8,128)(2,1)} %bitcast.83, bf16[2048,1024]{1,0:T(8,128)(2,1)} %all-gather.3.cloned.1.call-done), kind=kOutput, calls=%fused_computation.67 | convolution fusion | flops 1342177280 | bytes 7471104 | tf_op jit(solution)/shard_map/dot_general | solution.py:22
  325.5 4.9 %multiply_reduce_fusion.1 = (f32[320]{0:T(512)S(1)}, f32[320,2048]{1,0:T(8,128)S(1)}) fusion(f32[1280,2048]{1,0:T(8,128)} %convert_element_type.58, s32[]{:T(128)S(6)} %select_n.34, f32[320]{0:T(512)S(1)} %dynamic-slice.3, f32[2048]{0:T(1024)S(1)} %copy-done.16, f32[320,2048]{1,0:T(8,128)S(1)} %fusion.26, bf16[320,1024]{1,0:T(8,128)(2,1)S(1)} %bitcast.79, ...), kind=kOutput, calls=%fused_computation.14 | convolution fusion | flops 1345453824 | bytes 12724740 | tf_op jit(solution)/shard_map/dot_general | solution.py:22
  330.4 3.7 subtract_multiply_fusion
  334.1 49.4 %reduce-scatter.2.cloned.1.call-done = f32[32,256]{1,0:T(8,128)} async-done(((f32[2048,256]{1,0:T(8,128)}), f32[32,256]{1,0:T(8,128)}) %reduce-scatter.2.cloned.1.call-update) | async-done | bytes 32784 | tf_op jit(solution)/shard_map/reduce_scatter | solution.py:138
  (75 shorter events, 12.8 us)
Async XLA Ops:
  10.7 22.5 %all-to-all-start = ((s32[64,1,1]{2,1,0:T(1,128)}), s32[64,1,1]{2,1,0:T(1,128)S(1)}, u32[]{:S(2)}, u32[]{:S(2)}) async-start(s32[64,1,1]{2,1,0:T(1,128)} %copy.97), calls=%async_computation | async-start | bytes 65536 | tf_op jit(solution)/shard_map/all_to_all | solution.py:59
  23.8 4.0 %copy-start = (bf16[1280,2048]{1,0:T(8,128)(2,1)S(1)}, bf16[1280,2048]{1,0:T(8,128)(2,1)}, u32[]{:S(2)}) copy-start(bf16[1280,2048]{1,0:T(8,128)(2,1)} %param.16) | copy-start | bytes 15728644
  23.8 4.0 %copy-start.16 = (f32[2048]{0:T(1024)S(1)}, f32[2048]{0:T(1024)}, u32[]{:S(2)}) copy-start(f32[2048]{0:T(1024)} %param.17) | copy-start | bytes 24580
  27.9 3.0 copy-start.9
  99.9 8.1 %copy-start.13 = (bf16[1024,256]{1,0:T(8,128)(2,1)S(1)}, bf16[1024,256]{1,0:T(8,128)(2,1)}, u32[]{:S(2)}) copy-start(bf16[1024,256]{1,0:T(8,128)(2,1)} %param.13) | copy-start | bytes 1572868
  99.9 56.9 %all-to-all-start.1 = ((bf16[64,1,64,256]{3,2,1,0:T(8,128)(2,1)}), bf16[64,1,64,256]{3,2,1,0:T(8,128)(2,1)}, u32[]{:S(2)}, u32[]{:S(2)}) async-start(bf16[64,1,64,256]{3,2,1,0:T(8,128)(2,1)} %get-tuple-element.22), calls=%async_computation.1 | async-start | bytes 4194304 | tf_op jit(solution)/shard_map/all_to_all | solution.py:64
  107.2 1.0 copy-start.11
  107.2 1.2 copy-start.12
  107.2 214.3 %all-gather.3.cloned.1.call-start = ((), (), s32[]{:S(2)}) async-start(), calls=%async_computation.8 | async-start | bytes 5242880 | tf_op jit(solution)/shard_map/all_gather | solution.py:141
  108.4 54.3 %copy-start.1 = (bf16[8,128,2,128]{3,2,1,0:T(2,128)(2,1)}, bf16[8,128,2,128]{3,2,1,0:T(2,128)(2,1)S(1)}, u32[]{:S(2)}) copy-start(bf16[8,128,2,128]{3,2,1,0:T(2,128)(2,1)S(1)} %reshape.154) | copy-start | bytes 1572868
  109.2 55.6 %copy-start.14 = (bf16[8,128,2,128]{1,3,2,0:T(8,128)(2,1)}, bf16[8,128,2,128]{1,3,2,0:T(8,128)(2,1)S(1)}, u32[]{:S(2)}) copy-start(bf16[8,128,2,128]{1,3,2,0:T(8,128)(2,1)S(1)} %copy.103) | copy-start | bytes 1572868
  164.8 1.3 copy-start.7
  174.4 56.6 %all-to-all-start.5 = ((bf16[64,64,256]{2,1,0:T(8,128)(2,1)}), bf16[64,64,256]{2,1,0:T(8,128)(2,1)S(1)}, u32[]{:S(2)}, u32[]{:S(2)}) async-start(bf16[64,64,256]{2,1,0:T(8,128)(2,1)} %scatter_fusion.1), calls=%async_computation.5 | async-start | bytes 4194304 | tf_op jit(solution)/shard_map/all_to_all | solution.py:117
  181.3 144.2 %all-gather.5.cloned.1.call-start = ((), (), s32[]{:S(2)}) async-start(), calls=%async_computation.9 | async-start | bytes 5242880 | tf_op jit(solution)/shard_map/all_gather | solution.py:142
  187.8 2.7 copy-start.8
  187.8 3.0 copy-start.10
  187.8 3.1 copy-start.15
  190.9 1.6 copy-start.2
  191.5 1.0 copy-start.3
  231.0 56.8 %all-to-all-start.3 = ((bf16[64,64,256]{2,1,0:T(8,128)(2,1)}), bf16[64,64,256]{2,1,0:T(8,128)(2,1)}, u32[]{:S(2)}, u32[]{:S(2)}) async-start(bf16[64,64,256]{2,1,0:T(8,128)(2,1)} %scatter_fusion), calls=%async_computation.3 | async-start | bytes 4194304 | tf_op jit(solution)/shard_map/all_to_all | solution.py:116
  238.2 145.4 %reduce-scatter.2.cloned.1.call-start = ((), (), s32[]{:S(2)}) async-start(), calls=%async_computation.10 | async-start | bytes 2129920 | tf_op jit(solution)/shard_map/reduce_scatter | solution.py:138
  292.4 12.3 %all-to-all-start.4 = ((bf16[4,320,256]{2,1,0:T(8,128)(2,1)}), bf16[4,320,256]{2,1,0:T(8,128)(2,1)S(1)}, u32[]{:S(2)}, u32[]{:S(2)}) async-start(bf16[4,320,256]{2,1,0:T(8,128)(2,1)} %all_to_all.51), calls=%async_computation.4 | async-start | bytes 1310720 | tf_op jit(solution)/shard_map/all_to_all | solution.py:145
  304.7 4.4 %copy-start.5 = (bf16[4,320,256]{2,1,0:T(8,128)(2,1)}, bf16[4,320,256]{2,1,0:T(8,128)(2,1)S(1)}, u32[]{:S(2)}) copy-start(bf16[4,320,256]{2,1,0:T(8,128)(2,1)S(1)} %all-to-all-done.4) | copy-start | bytes 1966084
  304.7 15.6 %all-to-all-start.6 = ((bf16[4,320,256]{2,1,0:T(8,128)(2,1)}), bf16[4,320,256]{2,1,0:T(8,128)(2,1)}, u32[]{:S(2)}, u32[]{:S(2)}) async-start(bf16[4,320,256]{2,1,0:T(8,128)(2,1)} %all_to_all.56), calls=%async_computation.6 | async-start | bytes 1310720 | tf_op jit(solution)/shard_map/all_to_all | solution.py:146
  309.2 8.1 %copy-start.4 = (bf16[8,2,128,256]{2,3,1,0:T(8,128)(2,1)S(1)}, bf16[8,2,128,256]{2,3,1,0:T(8,128)(2,1)}, u32[]{:S(2)}) copy-start(bf16[8,2,128,256]{2,3,1,0:T(8,128)(2,1)} %copy-done.3) | copy-start | bytes 3145732
  317.7 1.7 copy-start.6
Sparse Core Ops, SparseCore 0:
  109.8 53.4 all-gather.2
  183.9 53.4 all-gather.4
Sparse Core Ops, SparseCore 1:
  246.5 137.0 reduce-scatter.1
where the time goes:
time: 397 us; the launch traced here: 391 us
  waiting for transfers between devices  171 us (43%)
  blocking collectives  59.4 us (15%)
  local copies, waits for them, and re-layouts  51.8 us (13%)
  starting transfers between devices  43.5 us (11%)
  matrix products  25.2 us (6%)
  other arithmetic  23.9 us (6%)
  between operations  15.9 us (4%)
    all_to_all x1, blocking collectives, passage_plan(): lax.all_to_all(picked_values, 'st', split_axis=0, concat_axis=0, tiled=True)  59.4 us
    reduce_scatter x1, waiting for transfers between devices, passage_plan(): lax.psum_scatter(weight_terms, 'st', scatter_dimension=0, tiled=True)  49.4 us
    all_to_all x1, waiting for transfers between devices, passage_plan(): lax.all_to_all(picked_keys, 'st', split_axis=0, concat_axis=0, tiled=True)  45.1 us
    all_to_all x1, waiting for transfers between devices, passage_plan(): lax.all_to_all(outgoing_keys, 'st', split_axis=0, concat_axis=0, tiled=True)  41.4 us
    all_to_all x1, waiting for transfers between devices, passage_plan(): lax.all_to_all(outgoing_values, 'st', split_axis=0, concat_axis=0, tiled=...  26.7 us
    all_to_all x1, starting transfers between devices, passage_plan(): lax.all_to_all(requests, 'st', split_axis=0, concat_axis=0, tiled=True)  13.1 us
    unnamed x40, local copies, waits for them, and re-layouts  10.7 us
    dot_general x2, matrix products, contract(): lax.dot_general(left, right, (((1,), (1,)), ((), ())), preferred_element_...  8.87 us
  transfers between devices with their start and end apart: 9, of which 6 were waited for; matrix products, arithmetic and copies ran while one was open for 22% of the time, Pallas kernels for 0%

commit v1 on v0

v1 whole, which is shorter than its diff:
```python
import functools

import jax
import jax.numpy as jnp
from jax import lax
from jax.experimental import pallas as pl
from jax.experimental.pallas import tpu as pltpu
from jax.sharding import PartitionSpec as P

HD = 128
PLEN = 64
EPS = 1e-06
NZ = 8
NJ = 8
NST = NZ * NJ
NTP = 4
MESH = pl.DeviceIdType.MESH
NT = (((1,), (1,)), ((), ()))
TN = (((0,), (0,)), ((), ()))
F32 = jnp.float32
BF16 = jnp.bfloat16


def dot(left, right, dims=(((1,), (0,)), ((), ()))):
    return lax.dot_general(left, right, dims, preferred_element_type=F32)


def row_scale(rows):
    return lax.rsqrt(jnp.mean(rows * rows, axis=-1, keepdims=True) + EPS)


def remote(src, dst, send_sem, recv_sem, axis, peer):
    return pltpu.make_async_remote_copy(
        src_ref=src, dst_ref=dst, send_sem=send_sem, recv_sem=recv_sem, device_id={axis: peer}, device_id_type=MESH
    )


def wait_bytes(ref, sem):
    pltpu.make_async_copy(ref, ref, sem).wait()


def greet(me, tp):
    z, j = me // NJ, me % NJ
    barrier = pltpu.get_barrier_semaphore()
    for t in range(1, NJ):
        pl.semaphore_signal(barrier, inc=1, device_id={"st": z * NJ + (j + t) % NJ}, device_id_type=MESH)
    for t in range(1, NZ):
        pl.semaphore_signal(barrier, inc=1, device_id={"st": (z + t) % NZ * NJ + j}, device_id_type=MESH)
    if tp is not None:
        for t in range(1, NTP):
            pl.semaphore_signal(barrier, inc=1, device_id={"tp": (tp + t) % NTP}, device_id_type=MESH)
    return barrier, NJ + NZ - 2 + (0 if tp is None else NTP - 1)


def table_kernel(owners, slots, store, gain, wk, wv, normed_out, kt, vt, meta, rows, normed, asked, in_sem, out_sem, ask_sem):
    me = lax.axis_index("st")
    z, j = me // NJ, me % NJ
    barrier, peers = greet(me, None)
    count = rows.shape[0] // 128

    def piece(i):
        return pl.ds(i * 128, 128)

    for i in range(count):
        pltpu.make_async_copy(store.at[piece(i)], rows.at[piece(i)], in_sem.at[i]).start()
    lane = lax.broadcasted_iota(jnp.int32, (1, 128), 1)
    request = jnp.full((1, 128), -1, jnp.int32)
    place = jnp.zeros((1, 128), jnp.int32)
    named = jnp.zeros((1, 128), jnp.int32)
    blocks, per_block = owners.shape
    for b in range(blocks):
        for i in range(per_block):
            at = b * per_block + i
            owner, slot = owners[b, i], slots[b, i]
            request = jnp.where(lane == owner, slot, request)
            place = jnp.where(lane == owner, at, place)
            named = jnp.where(lane == at, owner, named)
    asked[z, j] = request
    pl.semaphore_wait(barrier, peers)
    for t in range(1, NZ):
        far = (z + t) % NZ
        remote(asked.at[z, j], asked.at[z, j], ask_sem.at[0], ask_sem.at[1], "st", far * NJ + j).start()

    def project(i):
        at = piece(i)
        pltpu.make_async_copy(store.at[at], rows.at[at], in_sem.at[i]).wait()
        wide = rows[at].astype(F32)
        half = (wide * row_scale(wide) * gain[...]).astype(BF16)
        normed[at] = half
        kt[at] = dot(half, wk[...]).astype(BF16)
        vt[at] = dot(half, wv[...]).astype(BF16)
        pltpu.make_async_copy(normed.at[at], normed_out.at[at], out_sem.at[i]).start()

    for i in range(count // 2):
        project(i)
    wait_bytes(asked.at[pl.ds(0, NZ - 1), 0], ask_sem.at[1])
    for t in range(1, NJ):
        remote(asked.at[:, j], asked.at[:, j], ask_sem.at[2], ask_sem.at[3], "st", z * NJ + (j + t) % NJ).start()
    for i in range(count // 2, count):
        project(i)
    wait_bytes(asked.at[pl.ds(0, NJ - 1)], ask_sem.at[3])
    everyone = asked[...].reshape(NST, 128)
    lanes = lax.broadcasted_iota(jnp.int32, (NST, 128), 1)
    reader = lax.broadcasted_iota(jnp.int32, (NST, 128), 0)
    column = jnp.max(jnp.where(lanes == me, everyone, -1), axis=1, keepdims=True)
    across = jnp.max(jnp.where(lanes == reader, column, -1), axis=0, keepdims=True)
    before = jnp.max(jnp.where((reader < lanes) & (column == across), reader, -1), axis=0, keepdims=True)
    last = jnp.max(jnp.where(column == lanes, reader, -1), axis=0, keepdims=True)
    meta[0:1] = jnp.maximum(across, 0)
    meta[1:2] = jnp.where(before < 0, NST, before)
    meta[2:3] = jnp.where(last < 0, NST, last)
    meta[3:4] = place
    meta[4:5] = named
    meta[5:8] = jnp.zeros((3, 128), jnp.int32)
    wait_bytes(asked.at[pl.ds(0, NZ - 1), 0], ask_sem.at[0])
    wait_bytes(asked.at[pl.ds(0, NJ - 1)], ask_sem.at[2])
    for i in range(count):
        pltpu.make_async_copy(normed.at[piece(i)], normed_out.at[piece(i)], out_sem.at[i]).wait()


def tables(owners, slots, store, gain, w_key, w_value):
    rows, width = store.shape
    channels = w_key.shape[1]
    vmem = pl.BlockSpec(memory_space=pltpu.VMEM)
    smem = pl.BlockSpec(memory_space=pltpu.SMEM)
    far = pl.BlockSpec(memory_space=pltpu.HBM)
    return pl.pallas_call(
        table_kernel,
        out_shape=(
            jax.ShapeDtypeStruct((rows, width), BF16),
            jax.ShapeDtypeStruct((rows, channels), BF16),
            jax.ShapeDtypeStruct((rows, channels), BF16),
            jax.ShapeDtypeStruct((8, 128), jnp.int32),
        ),
        in_specs=[smem, smem, far, vmem, vmem, vmem],
        out_specs=(far, vmem, vmem, vmem),
        scratch_shapes=[
            pltpu.VMEM((rows, width), BF16),
            pltpu.VMEM((rows, width), BF16),
            pltpu.VMEM((NZ, NJ, 1, 128), jnp.int32),
            pltpu.SemaphoreType.DMA((rows // 128,)),
            pltpu.SemaphoreType.DMA((rows // 128,)),
            pltpu.SemaphoreType.DMA((4,)),
        ],
        cost_estimate=pl.CostEstimate(flops=3 * 10**9, bytes_accessed=10**7, transcendentals=0),
        compiler_params=pltpu.CompilerParams(collective_id=0, has_side_effects=True, vmem_limit_bytes=32 << 20),
        name="tables",
    )(owners, slots, store, gain, w_key, w_value)


TRANSIT = {(1, 2): 0, (1, 3): 8, (2, 3): 16, (1, 4): 24, (2, 4): 28, (3, 4): 32}
TRANSIT_PIECES = 36
ORDER = ((0, 4), (0, 3), (0, 2), (0, 1), (1, 4), (1, 3), (1, 2), (2, 4), (2, 3), (3, 4))


class Exchange:
    def __init__(self, me, number, x, column, transit, fin, z_send, z_recv, y_send, y_recv):
        self.z, self.j = me // NJ, me % NJ
        self.x, self.column, self.transit, self.fin = x, column.at[number], transit.at[number], fin
        self.z_send, self.z_recv = z_send.at[number], z_recv.at[number]
        self.y_send, self.y_recv = y_send.at[number], y_recv.at[number]

    def hop(self, side, g, d):
        s = 1 - 2 * side
        source = (self.z - s * g + NZ) % NZ
        dest = (source + s * d + NZ) % NZ
        first, count = (0, 8) if d < 4 else (4 * side, 4)
        if g == 0:
            src = self.x.at[pl.ds(dest * NJ + first, count)]
        else:
            src = self.transit.at[side, pl.ds(TRANSIT[g, d], count)]
        if g + 1 == d:
            dst = self.column.at[pl.ds(source * NJ + first, count)]
        else:
            dst = self.transit.at[side, pl.ds(TRANSIT[g + 1, d], count)]
        peer = (self.z + s + NZ) % NZ * NJ + self.j
        return remote(src, dst, self.z_send.at[side], self.z_recv.at[side, ORDER.index((g, d))], "st", peer)

    def send(self, *hops):
        for g, d in hops:
            for side in range(2):
                if g > 0:
                    self.hop(side, g - 1, d).wait_recv()
                self.hop(side, g, d).start()

    def spread(self, source, src):
        fin, z, j = self.fin, self.z, self.j
        pltpu.make_async_copy(src.at[source[0] * NJ + j], fin.at[source[1] * NJ + j], self.y_recv).start()

        @pl.loop(1, NJ)
        def _(t):
            other = (j + t) % NJ
            remote(src.at[source[0] * NJ + other], fin.at[source[1] * NJ + j], self.y_send, self.y_recv, "st", z * NJ + other).start()

    def spread_own(self):
        self.spread((self.z, self.z), self.x)

    def spread_from(self, d):
        for side in range(2):
            self.hop(side, d - 1, d).wait_recv()
        for side in range(1 if d == 4 else 2):
            source = (self.z - (1 - 2 * side) * d + NZ) % NZ
            self.spread((source, source), self.column)

    def arrive(self):
        wait_bytes(self.fin, self.y_recv)

    def finish(self):
        for side in range(2):
            wait_bytes(self.x, self.z_send.at[side])
        wait_bytes(self.fin.at[pl.ds(0, NZ * (NJ - 1))], self.y_send)


def main_kernel(
    meta, q_in, gate_in, cot_in, store_in, normed_in, wk_in, wv_in, gain, kt, vt,
    dq_ref, gs_ref, gw_ref,
    q, g, gate, x, column, transit, fin_k, fin_v, fin_b, weights, terms, stage, pv, wide_w, own, nrm, gwb, rs1, rsb, rs2, own_rows,
    z_send, z_recv, y_send, y_recv, in_sem, tp_sem, w_sem, rs_sem, nrm_sem,
):
    me = lax.axis_index("st")
    tp = lax.axis_index("tp")
    z, j = me // NJ, me % NJ
    core = me % 2
    scale = HD ** (-0.5)
    heads = q.shape[1] // HD
    width = q.shape[1]
    blocks = weights.shape[0]
    quarter = own.shape[1]
    barrier, peers = greet(me, tp)
    fins = (fin_k, fin_v, fin_b.at[0], fin_b.at[1])
    trips = [Exchange(me, n, x.at[n], column, transit, fins[n], z_send, z_recv, y_send, y_recv) for n in range(4)]
    ek, ev, bv, bk = trips
    mine = pl.ds(pl.multiple_of(tp * width, 128), width)

    loads = [
        pltpu.make_async_copy(q_in, q, in_sem.at[0]),
        pltpu.make_async_copy(cot_in, g, in_sem.at[1]),
        pltpu.make_async_copy(gate_in, gate, in_sem.at[2]),
        pltpu.make_async_copy(wk_in, wide_w.at[0, :, mine], in_sem.at[3]),
        pltpu.make_async_copy(wv_in, wide_w.at[1, :, mine], in_sem.at[4]),
        pltpu.make_async_copy(store_in.at[pl.ds(pl.multiple_of(tp * quarter, 16), quarter)], own_rows, in_sem.at[5]),
    ]
    for load in loads:
        load.start()

    def pick(table, number):
        @pl.loop(0, NST)
        def _(r):
            x[number, r] = table[meta[0, r]]

    pick(kt, 0)
    pl.semaphore_wait(barrier, peers)
    ek.send((0, 4), (0, 3), (0, 2), (0, 1))
    ek.spread_own()
    pick(vt, 1)

    part = wide_w.shape[1] // 2
    half = pl.ds(pl.multiple_of(core * part, 16), part)
    for load in loads[3:5]:
        load.wait()

    def weight_move(number, away):
        ref = wide_w.at[number, half, mine]
        return remote(ref, ref, w_sem.at[0, number, away], w_sem.at[1, number, away], "tp", (tp + away) % NTP)

    def weight_pass(number, away):
        ref = wide_w.at[number, half, pl.ds(pl.multiple_of((tp + NTP - away) % NTP * width, 128), width)]
        return remote(ref, ref, w_sem.at[2, number, away], w_sem.at[3, number, away], "st", me + 1 - 2 * core)

    for number in range(2):
        for away in range(1, NTP):
            weight_move(number, away).start()

    ek.send((1, 4), (1, 3), (1, 2))
    ek.spread_from(1)
    ek.send((2, 4), (2, 3))
    ek.spread_from(2)
    ev.send((0, 4), (0, 3))
    ek.send((3, 4))
    ev.send((0, 2), (0, 1))
    ev.spread_own()
    ek.spread_from(3)
    ek.spread_from(4)

    for load in loads[:3]:
        load.wait()

    @pl.loop(0, blocks)
    def _(b):
        at = pl.ds(b * 128, 128)
        g[at] = (jax.nn.sigmoid(gate[at].astype(F32)) * g[at].astype(F32)).astype(BF16)

    ek.arrive()

    def gathered(fin, b, cols):
        return jnp.concatenate([fin[meta[4, b * 4 + i], :, cols] for i in range(4)], axis=0)

    @pl.loop(0, blocks)
    def _(b):
        at = pl.ds(b * 128, 128)
        for h in range(heads):
            cols = pl.ds(h * HD, HD)
            score = dot(gathered(fin_k, b, cols), q[at, cols], NT) * scale
            raised = jnp.exp(score - jnp.max(score, axis=0, keepdims=True))
            weight = raised / jnp.sum(raised, axis=0, keepdims=True)
            weights[b, h] = weight
            terms[pl.ds(b * 4, 4), :, cols] = dot(weight.astype(BF16), g[at, cols]).astype(BF16).reshape(4, PLEN, HD)

    def order(number):
        @pl.loop(0, NST)
        def _(o):
            x[number, o] = terms[meta[3, o]]

    order(2)
    ev.send((1, 4), (1, 3), (1, 2))
    ev.spread_from(1)
    ev.send((2, 4), (2, 3))
    ev.spread_from(2)
    bv.send((0, 4), (0, 3))
    ev.send((3, 4))
    bv.send((0, 2), (0, 1))
    bv.spread_own()
    ev.spread_from(3)
    ev.spread_from(4)
    for number in range(2):
        for away in range(1, NTP):
            weight_move(number, away).wait_recv()
            weight_pass(number, away).start()
    ev.arrive()

    @pl.loop(0, blocks)
    def _(b):
        at = pl.ds(b * 128, 128)
        for h in range(heads):
            cols = pl.ds(h * HD, HD)
            steep = dot(gathered(fin_v, b, cols), g[at, cols], NT)
            weight = weights[b, h]
            delta = jnp.sum(weight.astype(BF16).astype(F32) * steep, axis=0, keepdims=True)
            slope = (weight * (steep - delta)).astype(BF16)
            terms[pl.ds(b * 4, 4), :, cols] = (dot(slope, q[at, cols]) * scale).astype(BF16).reshape(4, PLEN, HD)
            dq_ref[at, cols] = dot(slope, gathered(fin_k, b, cols), TN) * scale

    order(3)
    bv.send((1, 4), (1, 3), (1, 2))
    bv.spread_from(1)
    bv.send((2, 4), (2, 3))
    bv.spread_from(2)
    bk.send((0, 4), (0, 3))
    bv.send((3, 4))
    bk.send((0, 2), (0, 1))
    bk.spread_own()
    bv.spread_from(3)
    bv.spread_from(4)

    def normed_load(i):
        return pltpu.make_async_copy(normed_in.at[:, pl.ds(i * 256, 256)], nrm.at[i % 2], nrm_sem.at[i % 2])

    normed_load(0).start()
    stage[NST] = jnp.zeros(stage.shape[1:], F32)
    bv.arrive()

    def add_up(fin):
        for h in range(heads):
            cols = pl.ds(h * HD, HD)

            @pl.loop(0, NST)
            def _(r):
                stage[r] = fin[r, :, cols].astype(F32) + stage[meta[1, r]]

            @pl.loop(0, pv.shape[0] // PLEN)
            def _(p):
                pv[pl.ds(pl.multiple_of(p * PLEN, PLEN), PLEN), cols] = stage[meta[2, p]].astype(BF16)

    def across(number, away):
        src = pv.at[pl.ds(pl.multiple_of((tp + away) % NTP * quarter, 16), quarter)]
        return remote(src, own.at[number, :, mine], tp_sem.at[0, number, away], tp_sem.at[1, number, away], "tp", (tp + away) % NTP)

    def kept(number):
        src = pv.at[pl.ds(pl.multiple_of(tp * quarter, 16), quarter)]
        return pltpu.make_async_copy(src, own.at[number, :, mine], tp_sem.at[0, number, 0])

    add_up(fins[2])
    kept(1).start()
    for away in range(1, NTP):
        across(1, away).start()
    bk.send((1, 4), (1, 3), (1, 2))
    bk.spread_from(1)
    for i in range(NZ):
        if i + 1 < NZ:
            normed_load(i + 1).start()
        normed_load(i).wait()
        gwb[i] = dot(nrm[i % 2], pv[...], TN).astype(BF16).reshape(NJ, 32, width)
    for t in range(1, NJ):
        other = (j + t) % NJ
        remote(gwb.at[:, other], rs1.at[j], rs_sem.at[0], rs_sem.at[1], "st", z * NJ + other).start()
    bk.send((2, 4), (2, 3))
    bk.spread_from(2)
    bk.send((3, 4))
    wait_bytes(rs1.at[pl.ds(0, NJ - 1)], rs_sem.at[1])
    total = gwb[:, j].astype(F32)
    for t in range(1, NJ):
        total = total + rs1[(j + t) % NJ].astype(F32)
    rsb[...] = total.astype(BF16)
    gw_ref[...] = gwb[z, j].astype(F32)
    for t in range(1, NJ):
        gw_ref[...] += rs1[(j + t) % NJ, z].astype(F32)
    bk.spread_from(3)
    for t in range(1, NZ):
        other = (z + t) % NZ
        remote(rsb.at[other], rs2.at[z], rs_sem.at[2], rs_sem.at[3], "st", other * NJ + j).start()
    bk.spread_from(4)
    for number in range(2):
        for away in range(1, NTP):
            weight_pass(number, away).wait_recv()
    kept(1).wait()
    for away in range(1, NTP):
        across(1, away).wait()
    for i in range(8):
        out = pl.ds(i * 256, 256)
        gs_ref[:, out] = dot(own[1], wide_w[1, out], NT)
    wait_bytes(rs2.at[pl.ds(0, NZ - 1)], rs_sem.at[3])
    for t in range(1, NZ):
        gw_ref[...] += rs2[(z + t) % NZ].astype(F32)
    loads[5].wait()
    bk.arrive()
    add_up(fins[3])
    kept(0).start()
    for away in range(1, NTP):
        across(0, away).start()
    kept(0).wait()
    for away in range(1, NTP):
        across(0, away).wait()
    for i in range(8):
        out = pl.ds(i * 256, 256)
        gs_ref[:, out] += dot(own[0], wide_w[0, out], NT)

    @pl.loop(0, quarter // 32)
    def _(i):
        at = pl.ds(pl.multiple_of(i * 32, 32), 32)
        rows = own_rows[at].astype(F32)
        inverse = row_scale(rows)
        unit = rows * inverse
        grad_unit = gs_ref[at] * gain[...]
        gs_ref[at] = inverse * (grad_unit - unit * jnp.mean(grad_unit * unit, axis=-1, keepdims=True))

    for trip in trips:
        trip.finish()
    for number in range(2):
        for away in range(1, NTP):
            weight_move(number, away).wait_send()
            weight_pass(number, away).wait_send()
    wait_bytes(rs1.at[pl.ds(0, NJ - 1)], rs_sem.at[0])
    wait_bytes(rs2.at[pl.ds(0, NZ - 1)], rs_sem.at[2])


def attend(meta, queries, gate_pre, cotangent, store, normed, w_key, w_value, gain, key_table, value_table):
    tokens, width = queries.shape
    rows, features = store.shape
    heads = width // HD
    blocks = tokens // 128
    quarter = rows // NTP
    vmem = pl.BlockSpec(memory_space=pltpu.VMEM)
    smem = pl.BlockSpec(memory_space=pltpu.SMEM)
    far = pl.BlockSpec(memory_space=pltpu.HBM)
    piece = (PLEN, width)
    dma = pltpu.SemaphoreType.DMA
    return pl.pallas_call(
        main_kernel,
        out_shape=(
            jax.ShapeDtypeStruct((tokens, width), F32),
            jax.ShapeDtypeStruct((quarter, features), F32),
            jax.ShapeDtypeStruct((features // NST, width), F32),
        ),
        in_specs=[smem] + [far] * 7 + [vmem] * 3,
        out_specs=(vmem,) * 3,
        scratch_shapes=[
            pltpu.VMEM((tokens, width), BF16),
            pltpu.VMEM((tokens, width), BF16),
            pltpu.VMEM((tokens, width), BF16),
            pltpu.VMEM((4, NST) + piece, BF16),
            pltpu.VMEM((4, NST) + piece, BF16),
            pltpu.VMEM((4, 2, TRANSIT_PIECES) + piece, BF16),
            pltpu.VMEM((NST,) + piece, BF16),
            pltpu.VMEM((NST,) + piece, BF16),
            pltpu.VMEM((2, NST) + piece, BF16),
            pltpu.VMEM((blocks, heads, 256, 128), F32),
            pltpu.VMEM((blocks * 4,) + piece, BF16),
            pltpu.VMEM((NST + 1, PLEN, HD), F32),
            pltpu.VMEM((rows, width), BF16),
            pltpu.VMEM((2, features, width * NTP), BF16),
            pltpu.VMEM((2, quarter, width * NTP), BF16),
            pltpu.VMEM((2, rows, 256), BF16),
            pltpu.VMEM((NZ, NJ, features // NST, width), BF16),
            pltpu.VMEM((NJ, NZ, features // NST, width), BF16),
            pltpu.VMEM((NZ, features // NST, width), BF16),
            pltpu.VMEM((NZ, features // NST, width), BF16),
            pltpu.VMEM((quarter, features), BF16),
            dma((4, 2)),
            dma((4, 2, len(ORDER))),
            dma((4,)),
            dma((4,)),
            dma((6,)),
            dma((2, 2, NTP)),
            dma((4, 2, NTP)),
            dma((4,)),
            dma((2,)),
        ],
        cost_estimate=pl.CostEstimate(flops=10**10, bytes_accessed=10**7, transcendentals=0),
        compiler_params=pltpu.CompilerParams(collective_id=1, has_side_effects=True, vmem_limit_bytes=67043328),
        name="attend",
    )(meta, queries, gate_pre, cotangent, store, normed, w_key, w_value, gain, key_table, value_table)


def local(queries, gate_pre, cotangent, store, store_gain, w_key, w_value, owners, slots):
    gain = store_gain[None]
    normed, key_table, value_table, meta = tables(owners, slots, store, gain, w_key, w_value)
    key_table, value_table = (table.reshape(-1, PLEN, table.shape[1]) for table in (key_table, value_table))
    grad_queries, grad_store, grad_w_value = attend(
        meta, queries, gate_pre, cotangent, store, normed, w_key, w_value, gain, key_table, value_table
    )
    return (grad_queries, grad_store, grad_w_value)


def solution(mesh):
    placed = (
        P("st", "tp"),
        P("st", "tp"),
        P("st", "tp"),
        P("st", None),
        P(),
        P(None, "tp"),
        P(None, "tp"),
        P("st", None),
        P("st", None),
    )
    return jax.shard_map(
        local,
        mesh=mesh,
        in_specs=placed,
        out_specs=(P("st", "tp"), P(("st", "tp"), None), P("st", "tp")),
        check_vma=False,
    )
```

time: 397 us -> 255 us (0.64); the launches traced: 391 us -> 254 us
  Pallas kernels: 0 us -> 236 us
  waiting for transfers between devices: 171 us -> 0 us
  blocking collectives: 59.4 us -> 0 us
  starting transfers between devices: 43.5 us -> 0 us
  local copies, waits for them, and re-layouts: 51.8 us -> 18.1 us
  matrix products: 25.2 us -> 0 us
  other arithmetic: 23.9 us -> 0 us
  between operations: 15.9 us -> 0.67 us
    pallas_call x0 -> x2, Pallas kernels: none -> 236 us  [the longest x1 218 us: attend(): pl.pallas_call(main_kernel, out_shape=(jax.ShapeDtypeStruct((tokens, widt...]
    all_to_all x6 -> x0, waiting for transfers between devices: 121 us -> none  [the longest x1 45.1 us: passage_plan(): lax.all_to_all(picked_keys, 'st', split_axis=0, concat_axis=0, tiled=True)]
    all_to_all x1 -> x0, blocking collectives: 59.4 us -> none  [passage_plan(): lax.all_to_all(picked_values, 'st', split_axis=0, concat_axis=0, tiled=True)]
    reduce_scatter x1 -> x0, waiting for transfers between devices: 49.4 us -> none  [passage_plan(): lax.psum_scatter(weight_terms, 'st', scatter_dimension=0, tiled=True)]
    all_to_all x6 -> x0, starting transfers between devices: 42.9 us -> none  [the longest x1 13.1 us: passage_plan(): lax.all_to_all(requests, 'st', split_axis=0, concat_axis=0, tiled=True)]
    dot_general x13 -> x0, matrix products: 25.2 us -> none  [the longest x2 8.87 us: contract(): lax.dot_general(left, right, (((1,), (1,)), ((), ())), preferred_element_...]
    scatter x2 -> x0, local copies, waits for them, and re-layouts: 9.98 us -> none  [the longest x1 5.29 us: passage_plan(): outgoing_keys = empty_slots.at[position].set(grad_keys.astype(jnp.bfloat16))]
    reshape x10 -> x0, local copies, waits for them, and re-layouts: 9.11 us -> none  [the longest x2 5.76 us: passage_plan(): mine_values = mine_values.reshape(blocks, span, local_heads, head_dim)]
  transfers between devices with their start and end apart: 9 -> 0, of which waited for: 6 -> 0; matrix products, arithmetic and copies ran while one was open for 22% -> 0% of each run, Pallas kernels for 0% -> 0%
where the time goes in v1:
time: 255 us; the launch traced here: 254 us
  Pallas kernels  236 us (93%)
  local copies, waits for them, and re-layouts  18.1 us (7%)
    pallas_call x1, Pallas kernels, attend(): pl.pallas_call(main_kernel, out_shape=(jax.ShapeDtypeStruct((tokens, widt...  218 us
    unnamed x23, local copies, waits for them, and re-layouts  18.1 us
    pallas_call x1, Pallas kernels, tables(): pl.pallas_call(table_kernel, out_shape=(jax.ShapeDtypeStruct((rows, width...  17.9 us

profile of v1, /device:TPU:1, one launch (start us, length us, event | category | flops | bytes accessed | tf_op | source)
XLA Modules:
  0.0 254.4 jit_solution(1041317521087587004)
XLA Ops:
  0.6 0.8 copy.12.owners
  1.4 0.8 copy.13.slots
  2.1 0.0 copy-start
  2.1 2.5 copy-done
  4.6 0.0 copy-start.1
  4.6 1.2 copy-done.1
  5.9 0.0 copy-start.2
  5.9 1.2 copy-done.2
  7.1 0.0 copy-start.3
  7.1 0.7 copy-done.3
  7.8 17.9 %tables.1 = (bf16[1280,2048]{1,0:T(8,128)(2,1)S(1)}, bf16[1280,256]{1,0:T(8,128)(2,1)S(1)}, bf16[1280,256]{1,0:T(8,128)(2,1)S(1)}, s32[8,128]{1,0:T(8,128)S(1)}) custom-call(s32[8,4]{1,0:T(8,128)S(1)} %copy.12.owners, s32[8,4]{1,0:T(8,128)S(1)} %copy.13.slots, bf16[1280,2048]{1,0:T(8,128)(2,1)S(1)} %copy-done, f32[1,2048]{1,0:T(1,128)S(1)} %bitcast.4, ...), custom_call_target="tpu_custom_call" | custom-call | flops 3000000000 | bytes 10000000 | tf_op jit(solution)/shard_map/tables/pallas_call | solution.py:127
  25.7 0.0 copy-start.4
  25.7 0.8 copy-done.4
  26.5 0.0 copy-start.5
  26.5 0.8 copy-done.5
  27.4 0.0 copy-start.6
  27.4 2.3 copy-done.6
  29.7 0.0 copy-start.7
  29.7 0.6 copy-done.7
  30.3 217.7 %attend.1 = (f32[1024,256]{1,0:T(8,128)}, f32[320,2048]{1,0:T(8,128)}, f32[32,256]{1,0:T(8,128)}) custom-call(s32[8,128]{1,0:T(8,128)} %copy-done.7, bf16[1024,256]{1,0:T(8,128)(2,1)} %q_in.1, bf16[1024,256]{1,0:T(8,128)(2,1)} %gate_in.1, bf16[1024,256]{1,0:T(8,128)(2,1)} %cot_in.1, bf16[1280,2048]{1,0:T(8,128)(2,1)} %store_in.1, ...), custom_call_target="tpu_custom_call" | custom-call | flops 10000000000 | bytes 10000000 | tf_op jit(solution)/shard_map/attend/pallas_call | solution.py:467
  248.0 0.0 copy-start.8
  248.0 2.3 copy.17
  250.3 3.5 %copy.18 = f32[320,2048]{1,0:T(8,128)} copy(f32[320,2048]{1,0:T(8,128)} %get-tuple-element.15) | data formatting | bytes 5242880
  253.8 0.0 copy-done.8
  253.8 0.6 copy.19
Async XLA Ops:
  2.1 2.5 copy-start
  4.6 1.2 copy-start.1
  5.9 1.2 copy-start.2
  7.1 0.7 copy-start.3
  25.7 0.8 copy-start.4
  26.5 0.8 copy-start.5
  27.4 2.3 copy-start.6
  29.7 0.6 copy-start.7
  248.0 5.8 %copy-start.8 = (f32[32,256]{1,0:T(8,128)S(1)}, f32[32,256]{1,0:T(8,128)}, u32[]{:S(2)}) copy-start(f32[32,256]{1,0:T(8,128)} %get-tuple-element.16) | copy-start | bytes 98308

commit v2 on v1

v2 whole, which is shorter than its diff:
```python
import functools

import jax
import jax.numpy as jnp
from jax import lax
from jax.experimental import pallas as pl
from jax.experimental.pallas import tpu as pltpu
from jax.sharding import PartitionSpec as P

HD = 128
PLEN = 64
EPS = 1e-06
NZ = 8
NJ = 8
NST = NZ * NJ
NTP = 4
MESH = pl.DeviceIdType.MESH
NT = (((1,), (1,)), ((), ()))
TN = (((0,), (0,)), ((), ()))
F32 = jnp.float32
BF16 = jnp.bfloat16


def dot(left, right, dims=(((1,), (0,)), ((), ()))):
    return lax.dot_general(left, right, dims, preferred_element_type=F32)


def row_scale(rows):
    return lax.rsqrt(jnp.mean(rows * rows, axis=-1, keepdims=True) + EPS)


def remote(src, dst, send_sem, recv_sem, axis, peer):
    return pltpu.make_async_remote_copy(
        src_ref=src, dst_ref=dst, send_sem=send_sem, recv_sem=recv_sem, device_id={axis: peer}, device_id_type=MESH
    )


def wait_bytes(ref, sem):
    pltpu.make_async_copy(ref, ref, sem).wait()


def greet(me, tp):
    z, j = me // NJ, me % NJ
    barrier = pltpu.get_barrier_semaphore()
    for t in range(1, NJ):
        pl.semaphore_signal(barrier, inc=1, device_id={"st": z * NJ + (j + t) % NJ}, device_id_type=MESH)
    for t in range(1, NZ):
        pl.semaphore_signal(barrier, inc=1, device_id={"st": (z + t) % NZ * NJ + j}, device_id_type=MESH)
    if tp is not None:
        for t in range(1, NTP):
            pl.semaphore_signal(barrier, inc=1, device_id={"tp": (tp + t) % NTP}, device_id_type=MESH)
    return barrier, NJ + NZ - 2 + (0 if tp is None else NTP - 1)


NY = NJ // 2


PASSAGES = 20
PART = PASSAGES // 2
BASE = 24
PREV, LAST, PLACE, NAMED, META_ROWS = 64, 68, 72, 73, 80


class Column:
    def __init__(self, me, via, z_send, z_recv, y_send, y_recv, via_send, via_recv):
        self.z, self.j, self.long, self.via = me // NJ, me % NJ, 1 - 2 * (me % 2), via
        self.z_send, self.z_recv, self.y_send, self.y_recv = z_send, z_recv, y_send, y_recv
        self.via_send, self.via_recv = via_send, via_recv

    def plane(self, steps):
        return (self.z + steps * self.long + NZ) % NZ

    def step(self, side, number, src, dst):
        peer = self.plane(1 - 2 * side) * NJ + self.j
        return remote(src, dst, self.z_send.at[side], self.z_recv.at[number], "st", peer)

    def beside(self, steps, core):
        return (self.j // 2 + steps + NY) % NY * 2 + core

    def spread(self, src, dst, plane, recv_sem):
        z, j, core = self.z, self.j, self.j % 2
        pltpu.make_async_copy(src.at[plane * NJ + j], dst.at[plane * NJ + j], recv_sem).start()
        for way in range(2):
            peer = z * NJ + self.beside(1 - 2 * way, core)
            ref = src.at[plane * NJ + self.beside(2, way)]
            remote(ref, self.via.at[2 * plane + way], self.y_send, self.via_recv.at[2 * plane + way], "st", peer).start()
        for steps, to in ((1, 0), (1, 1), (-1, 0), (-1, 1), (0, 1 - core)):
            other = self.beside(steps, to)
            remote(src.at[plane * NJ + other], dst.at[plane * NJ + j], self.y_send, recv_sem, "st", z * NJ + other).start()

    def pass_on(self, dst, plane, recv_sem):
        for way in range(2):
            steps = 1 - 2 * way
            ref = self.via.at[2 * plane + way]
            wait_bytes(ref, self.via_recv.at[2 * plane + way])
            place = plane * NJ + self.beside(-steps, self.j % 2)
            remote(ref, dst.at[place], self.via_send, recv_sem, "st", self.z * NJ + self.beside(steps, way)).start()


class Outward(Column):
    def __init__(self, me, meta, table, near, far, picked, passed, column, fin, via, *sems):
        super().__init__(me, via, *sems)
        self.meta, self.table, self.near, self.far = meta, table, near, far
        self.picked, self.passed, self.column, self.fin = picked, passed, column, fin

    def launch(self, part, side):
        at = pl.ds(part * PART, PART)
        return self.step(side, 2 * side + part, self.table.at[at], self.near.at[side, at])

    def relay(self, part):
        at = pl.ds(part * PART, PART)
        return self.step(0, 4 + part, self.near.at[0, at], self.far.at[at])

    def hop(self, name):
        column, picked, passed, at = self.column, self.picked, self.passed, self.block
        return {
            "s2": lambda: self.step(1, 6, picked.at[0], column.at[at(self.plane(1))]),
            "s3": lambda: self.step(1, 7, picked.at[1], passed.at[1]),
            "s3b": lambda: self.step(1, 8, passed.at[1], column.at[at(self.plane(2))]),
            "l3": lambda: self.step(0, 9, picked.at[2], column.at[at(self.plane(-2))]),
            "l4": lambda: self.step(0, 10, picked.at[3], passed.at[0]),
            "l4b": lambda: self.step(0, 11, passed.at[0], column.at[at(self.plane(-3))]),
        }[name]()

    def block(self, plane):
        return pl.ds(plane * NJ, NJ)

    def pick(self, table, owner_plane, reader_plane, out, first):
        meta, owner = self.meta, owner_plane * NJ + self.j

        @pl.loop(0, NJ)
        def _(t):
            out[first + t] = table[jnp.maximum(meta[reader_plane * NJ + t, owner], 0)]

    def deliver(self, plane):
        self.spread(self.column, self.fin, plane, self.y_recv.at[0])

    def onward(self, *steps):
        for one in steps:
            self.pass_on(self.fin, self.plane(one), self.y_recv.at[0])

    def start(self, part):
        for side in range(2):
            self.launch(part, side).start()

    def own(self):
        self.pick(self.table, self.z, self.z, self.column, self.z * NJ)
        self.deliver(self.z)

    def first(self):
        for part in range(2):
            self.launch(part, 0).wait_recv()
            self.relay(part).start()
        for part in range(2):
            self.launch(part, 1).wait_recv()
        owner = self.plane(1)
        self.pick(self.near.at[1], owner, self.plane(-2), self.picked.at[1], 0)
        self.hop("s3").start()
        self.pick(self.near.at[1], owner, self.plane(-1), self.picked.at[0], 0)
        self.hop("s2").start()
        for owner, side in ((self.plane(-1), 0), (self.plane(1), 1)):
            self.pick(self.near.at[side], owner, self.z, self.column, owner * NJ)
            self.deliver(owner)

    def second(self):
        self.hop("s3").wait_recv()
        self.hop("s3b").start()
        for part in range(2):
            self.relay(part).wait_recv()
        owner = self.plane(-2)
        self.pick(self.far, owner, self.plane(2), self.picked.at[3], 0)
        self.hop("l4").start()
        self.pick(self.far, owner, self.plane(1), self.picked.at[2], 0)
        self.hop("l3").start()
        self.pick(self.far, owner, self.z, self.column, owner * NJ)
        self.deliver(owner)
        self.hop("s2").wait_recv()
        self.deliver(self.plane(2))

    def third(self):
        self.hop("l4").wait_recv()
        self.hop("l4b").start()
        self.hop("s3b").wait_recv()
        self.deliver(self.plane(3))
        self.hop("l3").wait_recv()
        self.deliver(self.plane(-3))

    def fourth(self):
        self.hop("l4b").wait_recv()
        self.deliver(self.plane(-4))

    def arrive(self):
        wait_bytes(self.fin, self.y_recv.at[0])

    def finish(self):
        wait_bytes(self.column, self.z_send.at[0])
        wait_bytes(self.column.at[pl.ds(0, 44)], self.z_send.at[1])
        wait_bytes(self.column.at[pl.ds(0, NZ * (NJ - 1))], self.y_send)
        wait_bytes(self.via, self.via_send)


class Homeward(Column):
    def __init__(self, me, meta, x, column, slots, sums, gained, stage, via, *sems):
        super().__init__(me, via, *sems)
        self.meta, self.x, self.column, self.slots = meta, x, column, slots
        self.sums, self.gained, self.stage = sums, gained, stage

    def block(self, plane):
        return pl.ds(plane * NJ, NJ)

    def hop(self, name):
        mine = lambda steps: self.column.at[self.block(self.plane(steps))]
        slots, sums, gained = self.slots, self.sums, self.gained
        return {
            "l4": lambda: self.step(1, 0, mine(-4), slots.at[0]),
            "l3": lambda: self.step(1, 1, mine(-3), slots.at[1]),
            "l4b": lambda: self.step(1, 2, slots.at[0], slots.at[2]),
            "l2": lambda: self.step(1, 3, sums.at[0], gained.at[0]),
            "l1": lambda: self.step(1, 4, sums.at[1], gained.at[1]),
            "s3": lambda: self.step(0, 5, mine(3), slots.at[3]),
            "s2": lambda: self.step(0, 6, mine(2), slots.at[4]),
            "s3b": lambda: self.step(0, 7, slots.at[3], slots.at[5]),
            "s1": lambda: self.step(0, 8, sums.at[2], gained.at[2]),
        }[name]()

    def start(self, *steps):
        for one in steps:
            plane = self.plane(one)
            self.spread(self.x, self.column, plane, self.y_recv.at[plane])

    def onward(self, *steps):
        for one in steps:
            plane = self.plane(one)
            self.pass_on(self.column, plane, self.y_recv.at[plane])

    def gathered(self, steps):
        plane = self.plane(steps)
        wait_bytes(self.column.at[self.block(plane)], self.y_recv.at[plane])

    def add_up(self, combo, planes, slots, bases, store):
        meta, stage = self.meta, self.stage
        width = self.x.shape[-1]
        for first in range(0, width, HD):
            cols = pl.ds(first, HD)

            @pl.loop(0, PASSAGES)
            def _(p):
                total = jnp.zeros(stage.shape[1:], F32)
                for base in bases:
                    total = total + base[p, :, cols].astype(F32)
                stage[BASE + p] = total

            for rank, (plane, (ref, start)) in enumerate(zip(planes, slots)):

                @pl.loop(0, NJ)
                def _(t):
                    stage[rank * NJ + t] = ref[start + t, :, cols].astype(F32) + stage[meta[PREV + combo, plane * NJ + t]]

            @pl.loop(0, PASSAGES)
            def _(p):
                store(p, cols, stage[meta[LAST + combo, p]].astype(BF16))

    def into(self, number):
        def store(p, cols, value):
            self.sums[number, p, :, cols] = value

        return store

    def first(self):
        self.gathered(-4)
        self.hop("l4").start()
        self.gathered(3)
        self.hop("s3").start()
        self.gathered(-3)
        self.hop("l3").start()
        self.gathered(2)
        self.hop("s2").start()

    def second(self):
        self.hop("l4").wait_recv()
        self.hop("l4b").start()
        self.hop("s3").wait_recv()
        self.hop("s3b").start()

    def third(self):
        self.gathered(-2)
        self.hop("l3").wait_recv()
        self.hop("l4b").wait_recv()
        planes = (self.plane(2), self.plane(1), self.z)
        slots = ((self.slots.at[2], 0), (self.slots.at[1], 0), (self.column, self.plane(-2) * NJ))
        self.add_up(0, planes, slots, (), self.into(0))
        self.hop("l2").start()
        self.gathered(1)
        self.hop("s2").wait_recv()
        self.hop("s3b").wait_recv()
        planes = (self.plane(-2), self.plane(-1), self.z)
        slots = ((self.slots.at[5], 0), (self.slots.at[4], 0), (self.column, self.plane(1) * NJ))
        self.add_up(2, planes, slots, (), self.into(2))
        self.hop("s1").start()

    def fourth(self):
        self.gathered(-1)
        self.hop("l2").wait_recv()
        slots = ((self.column, self.plane(-1) * NJ),)
        self.add_up(1, (self.z,), slots, (self.gained.at[0],), self.into(1))
        self.hop("l1").start()

    def collect(self, store):
        self.gathered(0)
        self.hop("l1").wait_recv()
        self.hop("s1").wait_recv()
        slots = ((self.column, self.z * NJ),)
        self.add_up(3, (self.z,), slots, (self.gained.at[1], self.gained.at[2]), store)

    def finish(self):
        wait_bytes(self.column, self.z_send.at[1])
        wait_bytes(self.column.at[pl.ds(0, 44)], self.z_send.at[0])
        wait_bytes(self.column.at[pl.ds(0, NZ * (NJ - 1))], self.y_send)
        wait_bytes(self.via, self.via_send)


def plans(asked, me, place, named, meta):
    z, j, long = me // NJ, me % NJ, 1 - 2 * (me % 2)
    everyone = asked[...].reshape(NST, 128)
    meta[0:NST] = everyone
    lanes = lax.broadcasted_iota(jnp.int32, (NST, 128), 1)
    reader = lax.broadcasted_iota(jnp.int32, (NST, 128), 0)
    combos = ((-2, 2, 3, -1), (-1, 0, 1, -1), (1, -2, 3, 1), (0, 0, 1, 1))
    for number, (owner, start, count, way) in enumerate(combos):
        owner = (z + owner * long + NZ) % NZ * NJ + j
        start = (z + start * long + NZ) % NZ

        def rank(index):
            return ((index // NJ - start) * (way * long) + 2 * NZ) % NZ * NJ + index % NJ

        mine, other = rank(reader), rank(lanes)
        column = jnp.max(jnp.where(lanes == owner, everyone, -1), axis=1, keepdims=True)
        across = jnp.max(jnp.where(lanes == reader, column, -1), axis=0, keepdims=True)
        inside = mine < count * NJ
        before = jnp.max(jnp.where(inside & (mine < other) & (column == across), mine, -1), axis=0, keepdims=True)
        last = jnp.max(jnp.where(inside & (column == lanes), mine, -1), axis=0, keepdims=True)
        spot = lax.broadcasted_iota(jnp.int32, (1, 128), 1)
        meta[PREV + number : PREV + number + 1] = jnp.where(before < 0, BASE + jnp.maximum(across, 0), before)
        meta[LAST + number : LAST + number + 1] = jnp.where(last < 0, BASE + spot, last)
    meta[PLACE : PLACE + 1] = place
    meta[NAMED : NAMED + 1] = named
    meta[NAMED + 1 : META_ROWS] = jnp.zeros((META_ROWS - NAMED - 1, 128), jnp.int32)


def kernel(
    owners, slots, q_in, gate_in, cot_in, store_in, wk_in, wv_in, gain,
    dq_out, gs_out, gw_ref,
    rows, tables, asked, plan, meta, q, g, near_k, near_v, far_k, far_v, picked, passed, out_column, out_via, fin_k, fin_v, x, column, via_v, slot_v, sum_v, gain_v,
    xk, columnk, via_k, slot_k, sum_k, gain_k, weights, terms, stage, pv, pk, wide_w, own, gwb, rs1, rsb, rs2, gs,
    oz_send, oz_recv, oy_send, oy_recv, ov_send, ov_recv, hz_send, hz_recv, hy_send, hy_recv, hv_send, hv_recv,
    row_sem, ask_sem, in_sem, tp_sem, w_sem, rs_sem, out_sem,
):
    me = lax.axis_index("st")
    tp = lax.axis_index("tp")
    z, j = me // NJ, me % NJ
    core = me % 2
    scale = HD ** (-0.5)
    heads = q.shape[1] // HD
    width = q.shape[1]
    blocks = weights.shape[0]
    quarter = gs.shape[0]
    barrier, peers = greet(me, tp)
    slim = pl.ds(pl.multiple_of(tp * HD, HD), HD)

    def out_sems(n):
        return oz_send.at[n], oz_recv.at[n], oy_send.at[n], oy_recv.at[n], ov_send.at[n], ov_recv.at[n]

    def home_sems(n):
        return hz_send.at[n], hz_recv.at[n], hy_send.at[n], hy_recv.at[n], hv_send.at[n], hv_recv.at[n]

    fins = (fin_k, fin_v)
    ek, ev = (
        Outward(me, meta, tables.at[n], (near_k, near_v)[n], (far_k, far_v)[n], picked.at[n], passed.at[n], out_column.at[n], fins[n], out_via.at[n], *out_sems(n))
        for n in range(2)
    )
    bv = Homeward(me, meta, x, column, slot_v, sum_v, gain_v, stage, via_v, *home_sems(0))
    bk = [
        Homeward(me, meta, xk.at[h], columnk.at[h], slot_k.at[h], sum_k.at[h], gain_k.at[h], stage, via_k.at[h], *home_sems(1 + h))
        for h in range(2)
    ]

    weight_loads = [
        pltpu.make_async_copy(ref.at[:, :, pl.ds(h * HD, HD)], wide_w.at[n, h, :, :, slim], in_sem.at[2 * n + h])
        for n, ref in enumerate((wk_in, wv_in))
        for h in range(2)
    ]
    first_loads = [
        pltpu.make_async_copy(ref, x.at[pl.ds(n * NST // 2, NST // 2)], in_sem.at[7 + n])
        for n, ref in enumerate((wk_in, wv_in))
    ]
    token_loads = [
        pltpu.make_async_copy(q_in, q, in_sem.at[4]),
        pltpu.make_async_copy(cot_in, g, in_sem.at[5]),
        pltpu.make_async_copy(gate_in, pv.at[pl.ds(0, gate_in.shape[0])], in_sem.at[6]),
    ]
    count = rows.shape[0] // 256

    def chunk(i):
        return pl.ds(i * 256, 256)

    def row_load(i):
        return pltpu.make_async_copy(store_in.at[chunk(i)], rows.at[chunk(i)], row_sem.at[i])

    row_load(0).start()
    for load in first_loads:
        load.start()
    for i in range(1, count):
        row_load(i).start()
    for load in weight_loads + token_loads:
        load.start()

    lane = lax.broadcasted_iota(jnp.int32, (1, 128), 1)
    request = jnp.full((1, 128), -1, jnp.int32)
    place = jnp.zeros((1, 128), jnp.int32)
    named = jnp.zeros((1, 128), jnp.int32)
    per_block = owners.shape[0]
    for b in range(blocks):
        for i in range(per_block):
            at = b * per_block + i
            owner, slot = owners[i, b], slots[i, b]
            request = jnp.where(lane == owner, slot, request)
            place = jnp.where(lane == owner, at, place)
            named = jnp.where(lane == at, owner, named)
    asked[z, j] = request
    for load in first_loads:
        load.wait()

    def project(i):
        at = chunk(i)
        row_load(i).wait()

        @pl.loop(0, 8)
        def _(t):
            tile = pl.ds(i * 256 + t * 32, 32)
            raw = rows[tile].astype(F32)
            rows[tile] = (raw * row_scale(raw) * gain[...]).astype(BF16)

        for n in range(2):
            weight = x[pl.ds(n * NST // 2, NST // 2)].reshape(rows.shape[1], width)
            tables[n, pl.ds(4 * i, 4)] = dot(rows[at], weight).astype(BF16).reshape(4, PLEN, width)

    project(0)
    project(1)
    project(2)
    pl.semaphore_wait(barrier, peers)
    for t in range(1, NZ):
        other = (z + t) % NZ
        remote(asked.at[z, j], asked.at[z, j], ask_sem.at[0], ask_sem.at[1], "st", other * NJ + j).start()
    ek.start(0)
    project(3)
    project(4)
    ek.start(1)
    wait_bytes(asked.at[pl.ds(0, NZ - 1), 0], ask_sem.at[1])
    for t in range(1, NJ):
        remote(asked.at[:, j], asked.at[:, j], ask_sem.at[2], ask_sem.at[3], "st", z * NJ + (j + t) % NJ).start()
    ev.start(0)
    ev.start(1)

    part = wide_w.shape[2] // 2
    half_rows = pl.ds(core * part, part)

    def weight_move(n, away):
        ref = wide_w.at[n, :, half_rows, :, slim]
        return remote(ref, ref, w_sem.at[0, n, away], w_sem.at[1, n, away], "tp", (tp + away) % NTP)

    def weight_pass(n, away):
        ref = wide_w.at[n, :, half_rows, :, pl.ds(pl.multiple_of((tp + NTP - away) % NTP * HD, HD), HD)]
        return remote(ref, ref, w_sem.at[2, n, away], w_sem.at[3, n, away], "st", me + 1 - 2 * core)

    for load in weight_loads:
        load.wait()
    for n in range(2):
        for away in range(1, NTP):
            weight_move(n, away).start()
    wait_bytes(asked.at[pl.ds(0, NJ - 1)], ask_sem.at[3])
    plans(asked, me, place, named, plan)
    sent_plan = pltpu.make_async_copy(plan, meta, ask_sem.at[4])
    sent_plan.start()
    for load in token_loads:
        load.wait()

    @pl.loop(0, blocks)
    def _(b):
        at = pl.ds(b * 128, 128)
        g[at] = (jax.nn.sigmoid(pv[at].astype(F32)) * g[at].astype(F32)).astype(BF16)

    sent_plan.wait()
    ek.own()
    ek.first()
    ev.own()
    ek.onward(0, -1, 1)
    ek.second()
    ev.onward(0)
    ev.first()
    ek.onward(-2, 2)
    ek.third()
    ek.onward(3, -3)
    ek.fourth()
    ev.onward(-1, 1)
    ek.onward(-4)
    ek.arrive()

    def joined(n, b, cols):
        return jnp.concatenate([fins[n][meta[NAMED, b * 4 + i], :, cols] for i in range(4)], axis=0)

    @pl.loop(0, blocks)
    def _(b):
        at = pl.ds(b * 128, 128)
        for h in range(heads):
            cols = pl.ds(h * HD, HD)
            score = dot(joined(0, b, cols), q[at, cols], NT) * scale
            raised = jnp.exp(score - jnp.max(score, axis=0, keepdims=True))
            weight = raised / jnp.sum(raised, axis=0, keepdims=True)
            weight = weight.astype(BF16)
            weights[b, h] = weight
            terms[pl.ds(b * 4, 4), :, cols] = dot(weight, g[at, cols]).astype(BF16).reshape(4, PLEN, HD)

    @pl.loop(0, NST)
    def _(o):
        x[o] = terms[meta[PLACE, o]]

    bv.start(-4, 3, -3, 2, -2)
    ev.second()
    bv.onward(-4, 3, -3, 2, -2)
    ev.onward(-2, 2)
    ev.third()
    bv.first()
    ev.onward(3, -3)
    ev.fourth()
    bv.second()
    ev.onward(-4)
    bv.start(1, -1, 0)
    for n in range(2):
        for away in range(1, NTP):
            weight_move(n, away).wait_recv()
            weight_pass(n, away).start()
    ev.arrive()

    @pl.loop(0, blocks)
    def _(b):
        at = pl.ds(b * 128, 128)
        for h in range(heads):
            cols = pl.ds(h * HD, HD)
            steep = dot(joined(1, b, cols), g[at, cols], NT)
            weight = weights[b, h].astype(F32)
            delta = jnp.sum(weight * steep, axis=0, keepdims=True)
            slope = (weight * (steep - delta)).astype(BF16)
            terms[pl.ds(b * 4, 4), :, cols] = (dot(slope, q[at, cols]) * scale).astype(BF16).reshape(4, PLEN, HD)
            q[at, cols] = (dot(slope, joined(0, b, cols), TN) * scale).astype(BF16)

    dq_store = pltpu.make_async_copy(q, dq_out, out_sem.at[0])
    dq_store.start()

    @pl.loop(0, NST)
    def _(o):
        for h in range(2):
            xk[h, o] = terms[meta[PLACE, o], :, pl.ds(h * HD, HD)]

    bv.onward(1, -1, 0)
    bk[0].start(-4, 3, -3, 2, -2)
    bv.third()
    bk[0].onward(-4, 3, -3, 2, -2)
    bk[0].first()
    bk[0].start(1, -1, 0)
    bk[1].start(-4, 3, -3, 2, -2)
    bv.fourth()
    bk[0].onward(1, -1, 0)
    bk[1].onward(-4, 3, -3, 2, -2)
    bk[0].second()
    bk[1].first()
    bk[1].start(1, -1, 0)

    def keep(ref):
        def store(p, cols, value):
            ref[pl.ds(pl.multiple_of(p * PLEN, PLEN), PLEN), cols] = value

        return store

    bv.collect(keep(pv))

    def across(n, away):
        src = (pk.at[0], pk.at[1], pv.at[:, pl.ds(0, HD)], pv.at[:, pl.ds(HD, HD)])[n]
        peer = (tp + away) % NTP
        at = pl.ds(pl.multiple_of(peer * quarter, 16), quarter)
        return remote(src.at[at], own.at[n, :, slim], tp_sem.at[0, n, away], tp_sem.at[1, n, away], "tp", peer)

    def kept(n):
        src = (pk.at[0], pk.at[1], pv.at[:, pl.ds(0, HD)], pv.at[:, pl.ds(HD, HD)])[n]
        return pltpu.make_async_copy(src.at[pl.ds(pl.multiple_of(tp * quarter, 16), quarter)], own.at[n, :, slim], tp_sem.at[0, n, 0])

    def exchange(n):
        kept(n).start()
        for away in range(1, NTP):
            across(n, away).start()

    def exchanged(n):
        kept(n).wait()
        for away in range(1, NTP):
            across(n, away).wait()

    def weight_rows(n, h, i):
        return wide_w[n, h, 4 * i : 4 * i + 4].reshape(256, HD * NTP)

    exchange(2)
    exchange(3)
    bk[0].third()
    bk[1].onward(1, -1, 0)
    bk[1].second()
    for i in range(NZ):
        gwb[i] = dot(rows[:, i * 256 : (i + 1) * 256], pv[...], TN).astype(BF16).reshape(NJ, 32, width)
    own_rows = pltpu.make_async_copy(
        store_in.at[pl.ds(pl.multiple_of(tp * quarter, 16), quarter)], rows.at[pl.ds(0, quarter)], out_sem.at[1]
    )
    own_rows.start()
    for t in range(1, NJ):
        other = (j + t) % NJ
        remote(gwb.at[:, other], rs1.at[j], rs_sem.at[0], rs_sem.at[1], "st", z * NJ + other).start()
    bk[0].fourth()
    bk[1].third()
    wait_bytes(rs1.at[pl.ds(0, NJ - 1)], rs_sem.at[1])
    total = gwb[:, j].astype(F32)
    for t in range(1, NJ):
        total = total + rs1[(j + t) % NJ].astype(F32)
    rsb[...] = total.astype(BF16)
    gw_ref[...] = gwb[z, j].astype(F32)
    for t in range(1, NJ):
        gw_ref[...] += rs1[(j + t) % NJ, z].astype(F32)
    for t in range(1, NZ):
        other = (z + t) % NZ
        remote(rsb.at[other], rs2.at[z], rs_sem.at[2], rs_sem.at[3], "st", other * NJ + j).start()
    bk[0].collect(keep(pk.at[0]))
    exchange(0)
    bk[1].fourth()
    for n in range(2):
        for away in range(1, NTP):
            weight_pass(n, away).wait_recv()
    exchanged(2)
    exchanged(3)
    for i in range(8):
        out = pl.ds(i * 256, 256)
        gs[:, out] = dot(own[2], weight_rows(1, 0, i), NT) + dot(own[3], weight_rows(1, 1, i), NT)
    wait_bytes(rs2.at[pl.ds(0, NZ - 1)], rs_sem.at[3])
    for t in range(1, NZ):
        gw_ref[...] += rs2[(z + t) % NZ].astype(F32)
    exchanged(0)
    for i in range(8):
        out = pl.ds(i * 256, 256)
        gs[:, out] += dot(own[0], weight_rows(0, 0, i), NT)
    own_rows.wait()
    bk[1].collect(keep(pk.at[1]))
    exchange(1)
    exchanged(1)

    def stores(i):
        at = pl.ds(i * 64, 64)
        return pltpu.make_async_copy(rows.at[pl.ds(quarter + i * 64, 64)], gs_out.at[at], out_sem.at[2 + i])

    for i in range(8):
        out = pl.ds(i * 256, 256)
        gs[:, out] += dot(own[1], weight_rows(0, 1, i), NT)
    for i in range(quarter // 64):

        @pl.loop(0, 2)
        def _(t):
            at = pl.ds(i * 64 + t * 32, 32)
            raw = rows[at].astype(F32)
            inverse = row_scale(raw)
            unit = raw * inverse
            grad_unit = gs[at] * gain[...]
            slope = inverse * (grad_unit - unit * jnp.mean(grad_unit * unit, axis=-1, keepdims=True))
            rows[pl.ds(quarter + i * 64 + t * 32, 32)] = slope.astype(BF16)

        stores(i).start()

    for trip in (ek, ev, bv, *bk):
        trip.finish()
    for n in range(2):
        for away in range(1, NTP):
            weight_move(n, away).wait_send()
            weight_pass(n, away).wait_send()
    wait_bytes(asked.at[pl.ds(0, NZ - 1), 0], ask_sem.at[0])
    wait_bytes(asked.at[pl.ds(0, NJ - 1)], ask_sem.at[2])
    wait_bytes(rs1.at[pl.ds(0, NJ - 1)], rs_sem.at[0])
    wait_bytes(rs2.at[pl.ds(0, NZ - 1)], rs_sem.at[2])
    dq_store.wait()
    for i in range(quarter // 64):
        stores(i).wait()


def local(queries, gate_pre, cotangent, store, store_gain, w_key, w_value, owners, slots):
    tokens, width = queries.shape
    rows, features = store.shape
    heads = width // HD
    blocks = tokens // 128
    quarter = rows // NTP
    vmem = pl.BlockSpec(memory_space=pltpu.VMEM)
    smem = pl.BlockSpec(memory_space=pltpu.SMEM)
    far = pl.BlockSpec(memory_space=pltpu.HBM)
    piece = (PLEN, width)
    slim = (PLEN, HD)
    dma = pltpu.SemaphoreType.DMA
    grad_queries, grad_store, grad_w_value = pl.pallas_call(
        kernel,
        out_shape=(
            jax.ShapeDtypeStruct((tokens, width), BF16),
            jax.ShapeDtypeStruct((quarter, features), BF16),
            jax.ShapeDtypeStruct((features // NST, width), F32),
        ),
        in_specs=[smem, smem] + [far] * 6 + [vmem],
        out_specs=(far, far, vmem),
        scratch_shapes=[
            pltpu.VMEM((rows, features), BF16),
            pltpu.VMEM((2, PASSAGES) + piece, BF16),
            pltpu.VMEM((NZ, NJ, 1, 128), jnp.int32),
            pltpu.VMEM((META_ROWS, 128), jnp.int32),
            pltpu.SMEM((META_ROWS, 128), jnp.int32),
            pltpu.VMEM((tokens, width), BF16),
            pltpu.VMEM((tokens, width), BF16),
            pltpu.VMEM((2, PASSAGES) + piece, BF16),
            pltpu.VMEM((2, PASSAGES) + piece, BF16),
            pltpu.VMEM((PASSAGES,) + piece, BF16),
            pltpu.VMEM((PASSAGES,) + piece, BF16),
            pltpu.VMEM((2, 4, NJ) + piece, BF16),
            pltpu.VMEM((2, 2, NJ) + piece, BF16),
            pltpu.VMEM((2, NST) + piece, BF16),
            pltpu.VMEM((2, 2 * NZ) + piece, BF16),
            pltpu.VMEM((NST,) + piece, BF16),
            pltpu.VMEM((NST,) + piece, BF16),
            pltpu.VMEM((NST,) + piece, BF16),
            pltpu.VMEM((NST,) + piece, BF16),
            pltpu.VMEM((2 * NZ,) + piece, BF16),
            pltpu.VMEM((6, NJ) + piece, BF16),
            pltpu.VMEM((3, PASSAGES) + piece, BF16),
            pltpu.VMEM((3, PASSAGES) + piece, BF16),
            pltpu.VMEM((2, NST) + slim, BF16),
            pltpu.VMEM((2, NST) + slim, BF16),
            pltpu.VMEM((2, 2 * NZ) + slim, BF16),
            pltpu.VMEM((2, 6, NJ) + slim, BF16),
            pltpu.VMEM((2, 3, PASSAGES) + slim, BF16),
            pltpu.VMEM((2, 3, PASSAGES) + slim, BF16),
            pltpu.VMEM((blocks, heads, 256, 128), BF16),
            pltpu.VMEM((blocks * 4,) + piece, BF16),
            pltpu.VMEM((BASE + PASSAGES,) + slim, F32),
            pltpu.VMEM((rows, width), BF16),
            pltpu.VMEM((2, rows, HD), BF16),
            pltpu.VMEM((2, 2, NST // 2, PLEN, HD * NTP), BF16),
            pltpu.VMEM((4, quarter, HD * NTP), BF16),
            pltpu.VMEM((NZ, NJ, features // NST, width), BF16),
            pltpu.VMEM((NJ, NZ, features // NST, width), BF16),
            pltpu.VMEM((NZ, features // NST, width), BF16),
            pltpu.VMEM((NZ, features // NST, width), BF16),
            pltpu.VMEM((quarter, features), F32),
            dma((2, 2)),
            dma((2, 12)),
            dma((2,)),
            dma((2, 1)),
            dma((2,)),
            dma((2, 2 * NZ)),
            dma((3, 2)),
            dma((3, 9)),
            dma((3,)),
            dma((3, NZ)),
            dma((3,)),
            dma((3, 2 * NZ)),
            dma((rows // 256,)),
            dma((5,)),
            dma((9,)),
            dma((2, 4, NTP)),
            dma((4, 2, NTP)),
            dma((4,)),
            dma((2 + quarter // 64,)),
        ],
        cost_estimate=pl.CostEstimate(flops=10**10, bytes_accessed=10**7, transcendentals=0),
        compiler_params=pltpu.CompilerParams(collective_id=0, has_side_effects=True, vmem_limit_bytes=67043328),
        name="passages",
    )(owners.T, slots.T, queries, gate_pre, cotangent, store, *(w.reshape(-1, PLEN, width) for w in (w_key, w_value)), store_gain[None])
    return (grad_queries.astype(F32), grad_store.astype(F32), grad_w_value)


def solution(mesh):
    placed = (
        P("st", "tp"),
        P("st", "tp"),
        P("st", "tp"),
        P("st", None),
        P(),
        P(None, "tp"),
        P(None, "tp"),
        P("st", None),
        P("st", None),
    )
    return jax.shard_map(
        local,
        mesh=mesh,
        in_specs=placed,
        out_specs=(P("st", "tp"), P(("st", "tp"), None), P("st", "tp")),
        check_vma=False,
    )
```

time: 255 us -> 219 us (0.86)
  Pallas kernels: 236 us -> 210 us
  local copies, waits for them, and re-layouts: 18.1 us -> 0.62 us
  other arithmetic: 0 us -> 4.22 us
    pallas_call x2 -> x1, Pallas kernels: 236 us -> 210 us  [local(): pl.pallas_call(kernel, out_shape=(jax.ShapeDtypeStruct((tokens, width), B...]
    unnamed x23 -> x5, local copies, waits for them, and re-layouts: 18.1 us -> 0.62 us
    convert_element_type x0 -> x2, other arithmetic: none -> 4.22 us  [local(): return (grad_queries.astype(F32), grad_store.astype(F32), grad_w_value)]
where the time goes in v2:
time: 219 us; the launch traced here: 216 us
  Pallas kernels  210 us (96%)
  other arithmetic  4.22 us (2%)
    pallas_call x1, Pallas kernels, local(): pl.pallas_call(kernel, out_shape=(jax.ShapeDtypeStruct((tokens, width), B...  210 us

profile of v2, /device:TPU:1, one launch (start us, length us, event | category | flops | bytes accessed | tf_op | source)
XLA Modules:
  0.0 216.0 jit_solution(4524535111292158482)
XLA Ops:
  0.6 210.5 %passages.1 = (bf16[1024,256]{1,0:T(8,128)(2,1)}, bf16[320,2048]{1,0:T(8,128)(2,1)}, f32[32,256]{1,0:T(8,128)}) custom-call(s32[4,8]{1,0:T(4,128)} %bitcast.8, s32[4,8]{1,0:T(4,128)} %bitcast.9, bf16[1024,256]{1,0:T(8,128)(2,1)} %q_in.1, bf16[1024,256]{1,0:T(8,128)(2,1)} %gate_in.1, bf16[1024,256]{1,0:T(8,128)(2,1)} %cot_in.1, bf16[1280,2048]{1,0:T(8,128)(2,1)} %store_in.1, ...), custom_call_target="tpu_custom_call" | custom-call | flops 10000000000 | bytes 10000000 | tf_op jit(solution)/shard_map/passages/pallas_call | solution.py:707
  211.1 0.0 copy-start
  211.1 0.0 copy-start.1
  211.1 3.2 %convert_element_type.7 = f32[320,2048]{1,0:T(8,128)} convert(bf16[320,2048]{1,0:T(8,128)(2,1)} %get-tuple-element.7) | non-fusion elementwise | flops 655360 | bytes 3932160 | tf_op jit(solution)/shard_map/convert_element_type | solution.py:782
  214.3 0.0 copy-done
  214.3 1.0 convert_element_type.6
  215.4 0.0 copy-done.1
  215.4 0.6 copy.13
Async XLA Ops:
  211.1 3.2 %copy-start = (bf16[1024,256]{1,0:T(8,128)(2,1)S(1)}, bf16[1024,256]{1,0:T(8,128)(2,1)}, u32[]{:S(2)}) copy-start(bf16[1024,256]{1,0:T(8,128)(2,1)} %get-tuple-element.6) | copy-start | bytes 1572868
  211.1 4.2 %copy-start.1 = (f32[32,256]{1,0:T(8,128)S(1)}, f32[32,256]{1,0:T(8,128)}, u32[]{:S(2)}) copy-start(f32[32,256]{1,0:T(8,128)} %get-tuple-element.14) | copy-start | bytes 98308

commit v3 on v2

--- a/solution.py
+++ b/solution.py
@@ -62,10 +62,9 @@
 
 
 class Column:
-    def __init__(self, me, via, z_send, z_recv, y_send, y_recv, via_send, via_recv):
-        self.z, self.j, self.long, self.via = me // NJ, me % NJ, 1 - 2 * (me % 2), via
+    def __init__(self, me, z_send, z_recv, y_send, y_recv):
+        self.z, self.j, self.long = me // NJ, me % NJ, 1 - 2 * (me % 2)
         self.z_send, self.z_recv, self.y_send, self.y_recv = z_send, z_recv, y_send, y_recv
-        self.via_send, self.via_recv = via_send, via_recv
 
     def plane(self, steps):
         return (self.z + steps * self.long + NZ) % NZ
@@ -80,26 +79,14 @@
     def spread(self, src, dst, plane, recv_sem):
         z, j, core = self.z, self.j, self.j % 2
         pltpu.make_async_copy(src.at[plane * NJ + j], dst.at[plane * NJ + j], recv_sem).start()
-        for way in range(2):
-            peer = z * NJ + self.beside(1 - 2 * way, core)
-            ref = src.at[plane * NJ + self.beside(2, way)]
-            remote(ref, self.via.at[2 * plane + way], self.y_send, self.via_recv.at[2 * plane + way], "st", peer).start()
-        for steps, to in ((1, 0), (1, 1), (-1, 0), (-1, 1), (0, 1 - core)):
+        for steps, to in ((2, 0), (2, 1), (1, 0), (-1, 0), (1, 1), (-1, 1), (0, 1 - core)):
             other = self.beside(steps, to)
             remote(src.at[plane * NJ + other], dst.at[plane * NJ + j], self.y_send, recv_sem, "st", z * NJ + other).start()
 
-    def pass_on(self, dst, plane, recv_sem):
-        for way in range(2):
-            steps = 1 - 2 * way
-            ref = self.via.at[2 * plane + way]
-            wait_bytes(ref, self.via_recv.at[2 * plane + way])
-            place = plane * NJ + self.beside(-steps, self.j % 2)
-            remote(ref, dst.at[place], self.via_send, recv_sem, "st", self.z * NJ + self.beside(steps, way)).start()
-
 
 class Outward(Column):
-    def __init__(self, me, meta, table, near, far, picked, passed, column, fin, via, *sems):
-        super().__init__(me, via, *sems)
+    def __init__(self, me, meta, table, near, far, picked, passed, column, fin, *sems):
+        super().__init__(me, *sems)
         self.meta, self.table, self.near, self.far = meta, table, near, far
         self.picked, self.passed, self.column, self.fin = picked, passed, column, fin
 
@@ -135,10 +122,6 @@
     def deliver(self, plane):
         self.spread(self.column, self.fin, plane, self.y_recv.at[0])
 
-    def onward(self, *steps):
-        for one in steps:
-            self.pass_on(self.fin, self.plane(one), self.y_recv.at[0])
-
     def start(self, part):
         for side in range(2):
             self.launch(part, side).start()
@@ -147,10 +130,11 @@
         self.pick(self.table, self.z, self.z, self.column, self.z * NJ)
         self.deliver(self.z)
 
+    def forward(self, part):
+        self.launch(part, 0).wait_recv()
+        self.relay(part).start()
+
     def first(self):
-        for part in range(2):
-            self.launch(part, 0).wait_recv()
-            self.relay(part).start()
         for part in range(2):
             self.launch(part, 1).wait_recv()
         owner = self.plane(1)
@@ -196,12 +180,11 @@
         wait_bytes(self.column, self.z_send.at[0])
         wait_bytes(self.column.at[pl.ds(0, 44)], self.z_send.at[1])
         wait_bytes(self.column.at[pl.ds(0, NZ * (NJ - 1))], self.y_send)
-        wait_bytes(self.via, self.via_send)
 
 
 class Homeward(Column):
-    def __init__(self, me, meta, x, column, slots, sums, gained, stage, via, *sems):
-        super().__init__(me, via, *sems)
+    def __init__(self, me, meta, x, column, slots, sums, gained, stage, *sems):
+        super().__init__(me, *sems)
         self.meta, self.x, self.column, self.slots = meta, x, column, slots
         self.sums, self.gained, self.stage = sums, gained, stage
 
@@ -227,11 +210,6 @@
         for one in steps:
             plane = self.plane(one)
             self.spread(self.x, self.column, plane, self.y_recv.at[plane])
-
-    def onward(self, *steps):
-        for one in steps:
-            plane = self.plane(one)
-            self.pass_on(self.column, plane, self.y_recv.at[plane])
 
     def gathered(self, steps):
         plane = self.plane(steps)
@@ -316,7 +294,6 @@
         wait_bytes(self.column, self.z_send.at[1])
         wait_bytes(self.column.at[pl.ds(0, 44)], self.z_send.at[0])
         wait_bytes(self.column.at[pl.ds(0, NZ * (NJ - 1))], self.y_send)
-        wait_bytes(self.via, self.via_send)
 
 
 def plans(asked, me, place, named, meta):
@@ -350,9 +327,9 @@
 def kernel(
     owners, slots, q_in, gate_in, cot_in, store_in, wk_in, wv_in, gain,
     dq_out, gs_out, gw_ref,
-    rows, tables, asked, plan, meta, q, g, near_k, near_v, far_k, far_v, picked, passed, out_column, out_via, fin_k, fin_v, x, column, via_v, slot_v, sum_v, gain_v,
-    xk, columnk, via_k, slot_k, sum_k, gain_k, weights, terms, stage, pv, pk, wide_w, own, gwb, rs1, rsb, rs2, gs,
-    oz_send, oz_recv, oy_send, oy_recv, ov_send, ov_recv, hz_send, hz_recv, hy_send, hy_recv, hv_send, hv_recv,
+    rows, tables, asked, plan, meta, q, g, near_k, near_v, far_k, far_v, picked, passed, out_column, fin_k, fin_v, x, column, slot_v, sum_v, gain_v,
+    xk, columnk, slot_k, sum_k, gain_k, weights, terms, stage, pv, pk, wide_w, own, gwb, rs1, rsb, rs2, gs,
+    oz_send, oz_recv, oy_send, oy_recv, hz_send, hz_recv, hy_send, hy_recv,
     row_sem, ask_sem, in_sem, tp_sem, w_sem, rs_sem, out_sem,
 ):
     me = lax.axis_index("st")
@@ -368,19 +345,19 @@
     slim = pl.ds(pl.multiple_of(tp * HD, HD), HD)
 
     def out_sems(n):
-        return oz_send.at[n], oz_recv.at[n], oy_send.at[n], oy_recv.at[n], ov_send.at[n], ov_recv.at[n]
+        return oz_send.at[n], oz_recv.at[n], oy_send.at[n], oy_recv.at[n]
 
     def home_sems(n):
-        return hz_send.at[n], hz_recv.at[n], hy_send.at[n], hy_recv.at[n], hv_send.at[n], hv_recv.at[n]
+        return hz_send.at[n], hz_recv.at[n], hy_send.at[n], hy_recv.at[n]
 
     fins = (fin_k, fin_v)
     ek, ev = (
-        Outward(me, meta, tables.at[n], (near_k, near_v)[n], (far_k, far_v)[n], picked.at[n], passed.at[n], out_column.at[n], fins[n], out_via.at[n], *out_sems(n))
+        Outward(me, meta, tables.at[n], (near_k, near_v)[n], (far_k, far_v)[n], picked.at[n], passed.at[n], out_column.at[n], fins[n], *out_sems(n))
         for n in range(2)
     )
-    bv = Homeward(me, meta, x, column, slot_v, sum_v, gain_v, stage, via_v, *home_sems(0))
+    bv = Homeward(me, meta, x, column, slot_v, sum_v, gain_v, stage, *home_sems(0))
     bk = [
-        Homeward(me, meta, xk.at[h], columnk.at[h], slot_k.at[h], sum_k.at[h], gain_k.at[h], stage, via_k.at[h], *home_sems(1 + h))
+        Homeward(me, meta, xk.at[h], columnk.at[h], slot_k.at[h], sum_k.at[h], gain_k.at[h], stage, *home_sems(1 + h))
         for h in range(2)
     ]
 
@@ -458,7 +435,9 @@
     wait_bytes(asked.at[pl.ds(0, NZ - 1), 0], ask_sem.at[1])
     for t in range(1, NJ):
         remote(asked.at[:, j], asked.at[:, j], ask_sem.at[2], ask_sem.at[3], "st", z * NJ + (j + t) % NJ).start()
+    ek.forward(0)
     ev.start(0)
+    ek.forward(1)
     ev.start(1)
 
     part = wide_w.shape[2] // 2
@@ -490,26 +469,21 @@
         g[at] = (jax.nn.sigmoid(pv[at].astype(F32)) * g[at].astype(F32)).astype(BF16)
 
     sent_plan.wait()
+    ek.first()
     ek.own()
-    ek.first()
+    ek.second()
+    ek.third()
+    ev.forward(0)
+    ev.forward(1)
+    ev.first()
+    ek.fourth()
     ev.own()
-    ek.onward(0, -1, 1)
-    ek.second()
-    ev.onward(0)
-    ev.first()
-    ek.onward(-2, 2)
-    ek.third()
-    ek.onward(3, -3)
-    ek.fourth()
-    ev.onward(-1, 1)
-    ek.onward(-4)
     ek.arrive()
 
     def joined(n, b, cols):
         return jnp.concatenate([fins[n][meta[NAMED, b * 4 + i], :, cols] for i in range(4)], axis=0)
 
-    @pl.loop(0, blocks)
-    def _(b):
+    def weigh(b):
         at = pl.ds(b * 128, 128)
         for h in range(heads):
             cols = pl.ds(h * HD, HD)
@@ -520,25 +494,24 @@
             weights[b, h] = weight
             terms[pl.ds(b * 4, 4), :, cols] = dot(weight, g[at, cols]).astype(BF16).reshape(4, PLEN, HD)
 
+    pl.loop(0, blocks // 4)(weigh)
+    ev.second()
+    pl.loop(blocks // 4, blocks)(weigh)
+
     @pl.loop(0, NST)
     def _(o):
         x[o] = terms[meta[PLACE, o]]
 
     bv.start(-4, 3, -3, 2, -2)
-    ev.second()
-    bv.onward(-4, 3, -3, 2, -2)
-    ev.onward(-2, 2)
     ev.third()
+    ev.fourth()
     bv.first()
-    ev.onward(3, -3)
-    ev.fourth()
-    bv.second()
-    ev.onward(-4)
     bv.start(1, -1, 0)
     for n in range(2):
         for away in range(1, NTP):
             weight_move(n, away).wait_recv()
             weight_pass(n, away).start()
+    bv.second()
     ev.arrive()
 
     @pl.loop(0, blocks)
@@ -561,16 +534,12 @@
         for h in range(2):
             xk[h, o] = terms[meta[PLACE, o], :, pl.ds(h * HD, HD)]
 
-    bv.onward(1, -1, 0)
     bk[0].start(-4, 3, -3, 2, -2)
     bv.third()
-    bk[0].onward(-4, 3, -3, 2, -2)
     bk[0].first()
     bk[0].start(1, -1, 0)
     bk[1].start(-4, 3, -3, 2, -2)
     bv.fourth()
-    bk[0].onward(1, -1, 0)
-    bk[1].onward(-4, 3, -3, 2, -2)
     bk[0].second()
     bk[1].first()
     bk[1].start(1, -1, 0)
@@ -609,7 +578,6 @@
     exchange(2)
     exchange(3)
     bk[0].third()
-    bk[1].onward(1, -1, 0)
     bk[1].second()
     for i in range(NZ):
         gwb[i] = dot(rows[:, i * 256 : (i + 1) * 256], pv[...], TN).astype(BF16).reshape(NJ, 32, width)
@@ -728,18 +696,15 @@
             pltpu.VMEM((2, 4, NJ) + piece, BF16),
             pltpu.VMEM((2, 2, NJ) + piece, BF16),
             pltpu.VMEM((2, NST) + piece, BF16),
-            pltpu.VMEM((2, 2 * NZ) + piece, BF16),
             pltpu.VMEM((NST,) + piece, BF16),
             pltpu.VMEM((NST,) + piece, BF16),
             pltpu.VMEM((NST,) + piece, BF16),
             pltpu.VMEM((NST,) + piece, BF16),
-            pltpu.VMEM((2 * NZ,) + piece, BF16),
             pltpu.VMEM((6, NJ) + piece, BF16),
             pltpu.VMEM((3, PASSAGES) + piece, BF16),
             pltpu.VMEM((3, PASSAGES) + piece, BF16),
             pltpu.VMEM((2, NST) + slim, BF16),
             pltpu.VMEM((2, NST) + slim, BF16),
-            pltpu.VMEM((2, 2 * NZ) + slim, BF16),
             pltpu.VMEM((2, 6, NJ) + slim, BF16),
             pltpu.VMEM((2, 3, PASSAGES) + slim, BF16),
             pltpu.VMEM((2, 3, PASSAGES) + slim, BF16),
@@ -759,14 +724,10 @@
             dma((2, 12)),
             dma((2,)),
             dma((2, 1)),
-            dma((2,)),
-            dma((2, 2 * NZ)),
             dma((3, 2)),
             dma((3, 9)),
             dma((3,)),
             dma((3, NZ)),
-            dma((3,)),
-            dma((3, 2 * NZ)),
             dma((rows // 256,)),
             dma((5,)),
             dma((9,)),

time: 219 us -> 204 us (0.932); the launches traced: 216 us -> 203 us
  Pallas kernels: 210 us -> 198 us
    pallas_call x1, Pallas kernels: 210 us -> 198 us  [local(): pl.pallas_call(kernel, out_shape=(jax.ShapeDtypeStruct((tokens, width), B...]
where the time goes in v3:
time: 204 us; the launch traced here: 203 us
  Pallas kernels  198 us (97%)
  other arithmetic  4.22 us (2%)
    pallas_call x1, Pallas kernels, local(): pl.pallas_call(kernel, out_shape=(jax.ShapeDtypeStruct((tokens, width), B...  198 us
    convert_element_type x2, other arithmetic, local(): return (grad_queries.astype(F32), grad_store.astype(F32), grad_w_value)  4.22 us

profile of v3, /device:TPU:1, one launch (start us, length us, event | category | flops | bytes accessed | tf_op | source)
XLA Modules:
  0.0 203.4 jit_solution(6171182090341427594)
XLA Ops:
  0.6 197.9 %passages.1 = (bf16[1024,256]{1,0:T(8,128)(2,1)}, bf16[320,2048]{1,0:T(8,128)(2,1)}, f32[32,256]{1,0:T(8,128)}) custom-call(s32[4,8]{1,0:T(4,128)} %bitcast.8, s32[4,8]{1,0:T(4,128)} %bitcast.9, bf16[1024,256]{1,0:T(8,128)(2,1)} %q_in.1, bf16[1024,256]{1,0:T(8,128)(2,1)} %gate_in.1, bf16[1024,256]{1,0:T(8,128)(2,1)} %cot_in.1, bf16[1280,2048]{1,0:T(8,128)(2,1)} %store_in.1, ...), custom_call_target="tpu_custom_call" | custom-call | flops 10000000000 | bytes 10000000 | tf_op jit(solution)/shard_map/passages/pallas_call | solution.py:675
  198.6 0.0 copy-start
  198.6 0.0 copy-start.1
  198.6 3.2 %convert_element_type.7 = f32[320,2048]{1,0:T(8,128)} convert(bf16[320,2048]{1,0:T(8,128)(2,1)} %get-tuple-element.7) | non-fusion elementwise | flops 655360 | bytes 3932160 | tf_op jit(solution)/shard_map/convert_element_type | solution.py:743
  201.8 0.0 copy-done
  201.8 1.0 convert_element_type.6
  202.8 0.0 copy-done.1
  202.8 0.6 copy.13
Async XLA Ops:
  198.6 3.2 %copy-start = (bf16[1024,256]{1,0:T(8,128)(2,1)S(1)}, bf16[1024,256]{1,0:T(8,128)(2,1)}, u32[]{:S(2)}) copy-start(bf16[1024,256]{1,0:T(8,128)(2,1)} %get-tuple-element.6) | copy-start | bytes 1572868
  198.6 4.2 %copy-start.1 = (f32[32,256]{1,0:T(8,128)S(1)}, f32[32,256]{1,0:T(8,128)}, u32[]{:S(2)}) copy-start(f32[32,256]{1,0:T(8,128)} %get-tuple-element.14) | copy-start | bytes 98308

commit v4 on v3

--- a/solution.py
+++ b/solution.py
@@ -198,13 +198,15 @@
             "l4": lambda: self.step(1, 0, mine(-4), slots.at[0]),
             "l3": lambda: self.step(1, 1, mine(-3), slots.at[1]),
             "l4b": lambda: self.step(1, 2, slots.at[0], slots.at[2]),
-            "l2": lambda: self.step(1, 3, sums.at[0], gained.at[0]),
-            "l1": lambda: self.step(1, 4, sums.at[1], gained.at[1]),
-            "s3": lambda: self.step(0, 5, mine(3), slots.at[3]),
-            "s2": lambda: self.step(0, 6, mine(2), slots.at[4]),
-            "s3b": lambda: self.step(0, 7, slots.at[3], slots.at[5]),
-            "s1": lambda: self.step(0, 8, sums.at[2], gained.at[2]),
+            "s3": lambda: self.step(0, 9, mine(3), slots.at[3]),
+            "s2": lambda: self.step(0, 10, mine(2), slots.at[4]),
+            "s3b": lambda: self.step(0, 11, slots.at[3], slots.at[5]),
         }[name]()
+
+    def summed(self, number, part):
+        at = pl.ds(part * PART, PART)
+        side = 0 if number == 2 else 1
+        return self.step(side, 3 + 2 * number + part, self.sums.at[number, at], self.gained.at[number, at])
 
     def start(self, *steps):
         for one in steps:
@@ -215,34 +217,38 @@
         plane = self.plane(steps)
         wait_bytes(self.column.at[self.block(plane)], self.y_recv.at[plane])
 
-    def add_up(self, combo, planes, slots, bases, store):
+    def chain(self, combo, planes, slots):
         meta, stage = self.meta, self.stage
-        width = self.x.shape[-1]
-        for first in range(0, width, HD):
-            cols = pl.ds(first, HD)
-
-            @pl.loop(0, PASSAGES)
+        for half in range(stage.shape[0]):
+            cols = pl.ds(half * HD, HD)
+            for rank, (plane, (ref, start)) in enumerate(zip(planes, slots)):
+
+                @pl.loop(0, NJ)
+                def _(t):
+                    before = stage[half, meta[PREV + combo, plane * NJ + t]]
+                    stage[half, rank * NJ + t] = ref[start + t, :, cols].astype(F32) + before
+
+    def close(self, combo, part, bases, store):
+        meta, stage = self.meta, self.stage
+        for half in range(stage.shape[0]):
+            cols = pl.ds(half * HD, HD)
+
+            @pl.loop(part * PART, part * PART + PART)
             def _(p):
-                total = jnp.zeros(stage.shape[1:], F32)
+                total = stage[half, meta[LAST + combo, p]]
                 for base in bases:
                     total = total + base[p, :, cols].astype(F32)
-                stage[BASE + p] = total
-
-            for rank, (plane, (ref, start)) in enumerate(zip(planes, slots)):
-
-                @pl.loop(0, NJ)
-                def _(t):
-                    stage[rank * NJ + t] = ref[start + t, :, cols].astype(F32) + stage[meta[PREV + combo, plane * NJ + t]]
-
-            @pl.loop(0, PASSAGES)
-            def _(p):
-                store(p, cols, stage[meta[LAST + combo, p]].astype(BF16))
-
-    def into(self, number):
+                store(p, cols, total.astype(BF16))
+
+    def ship(self, combo, number, base=None):
         def store(p, cols, value):
             self.sums[number, p, :, cols] = value
 
-        return store
+        for part in range(2):
+            if base is not None:
+                self.summed(base, part).wait_recv()
+            self.close(combo, part, () if base is None else (self.gained.at[base],), store)
+            self.summed(number, part).start()
 
     def first(self):
         self.gathered(-4)
@@ -266,29 +272,30 @@
         self.hop("l4b").wait_recv()
         planes = (self.plane(2), self.plane(1), self.z)
         slots = ((self.slots.at[2], 0), (self.slots.at[1], 0), (self.column, self.plane(-2) * NJ))
-        self.add_up(0, planes, slots, (), self.into(0))
-        self.hop("l2").start()
+        self.chain(0, planes, slots)
+        self.ship(0, 0)
+
+    def third_short(self):
         self.gathered(1)
         self.hop("s2").wait_recv()
         self.hop("s3b").wait_recv()
         planes = (self.plane(-2), self.plane(-1), self.z)
         slots = ((self.slots.at[5], 0), (self.slots.at[4], 0), (self.column, self.plane(1) * NJ))
-        self.add_up(2, planes, slots, (), self.into(2))
-        self.hop("s1").start()
+        self.chain(2, planes, slots)
+        self.ship(2, 2)
 
     def fourth(self):
         self.gathered(-1)
-        self.hop("l2").wait_recv()
-        slots = ((self.column, self.plane(-1) * NJ),)
-        self.add_up(1, (self.z,), slots, (self.gained.at[0],), self.into(1))
-        self.hop("l1").start()
+        self.chain(1, (self.z,), ((self.column, self.plane(-1) * NJ),))
+        self.ship(1, 1, 0)
 
     def collect(self, store):
         self.gathered(0)
-        self.hop("l1").wait_recv()
-        self.hop("s1").wait_recv()
-        slots = ((self.column, self.z * NJ),)
-        self.add_up(3, (self.z,), slots, (self.gained.at[1], self.gained.at[2]), store)
+        self.chain(3, (self.z,), ((self.column, self.z * NJ),))
+        for part in range(2):
+            self.summed(2, part).wait_recv()
+            self.summed(1, part).wait_recv()
+            self.close(3, part, (self.gained.at[1], self.gained.at[2]), store)
 
     def finish(self):
         wait_bytes(self.column, self.z_send.at[1])
@@ -316,9 +323,8 @@
         inside = mine < count * NJ
         before = jnp.max(jnp.where(inside & (mine < other) & (column == across), mine, -1), axis=0, keepdims=True)
         last = jnp.max(jnp.where(inside & (column == lanes), mine, -1), axis=0, keepdims=True)
-        spot = lax.broadcasted_iota(jnp.int32, (1, 128), 1)
-        meta[PREV + number : PREV + number + 1] = jnp.where(before < 0, BASE + jnp.maximum(across, 0), before)
-        meta[LAST + number : LAST + number + 1] = jnp.where(last < 0, BASE + spot, last)
+        meta[PREV + number : PREV + number + 1] = jnp.where(before < 0, BASE, before)
+        meta[LAST + number : LAST + number + 1] = jnp.where(last < 0, BASE, last)
     meta[PLACE : PLACE + 1] = place
     meta[NAMED : NAMED + 1] = named
     meta[NAMED + 1 : META_ROWS] = jnp.zeros((META_ROWS - NAMED - 1, 128), jnp.int32)
@@ -328,7 +334,7 @@
     owners, slots, q_in, gate_in, cot_in, store_in, wk_in, wv_in, gain,
     dq_out, gs_out, gw_ref,
     rows, tables, asked, plan, meta, q, g, near_k, near_v, far_k, far_v, picked, passed, out_column, fin_k, fin_v, x, column, slot_v, sum_v, gain_v,
-    xk, columnk, slot_k, sum_k, gain_k, weights, terms, stage, pv, pk, wide_w, own, gwb, rs1, rsb, rs2, gs,
+    xk, columnk, slot_k, sum_k, gain_k, weights, terms, stage, stage_k, pv, pk, wide_w, own, gwb, rs1, rsb, rs2, gs,
     oz_send, oz_recv, oy_send, oy_recv, hz_send, hz_recv, hy_send, hy_recv,
     row_sem, ask_sem, in_sem, tp_sem, w_sem, rs_sem, out_sem,
 ):
@@ -357,7 +363,7 @@
     )
     bv = Homeward(me, meta, x, column, slot_v, sum_v, gain_v, stage, *home_sems(0))
     bk = [
-        Homeward(me, meta, xk.at[h], columnk.at[h], slot_k.at[h], sum_k.at[h], gain_k.at[h], stage, *home_sems(1 + h))
+        Homeward(me, meta, xk.at[h], columnk.at[h], slot_k.at[h], sum_k.at[h], gain_k.at[h], stage_k.at[h], *home_sems(1 + h))
         for h in range(2)
     ]
 
@@ -436,9 +442,8 @@
     for t in range(1, NJ):
         remote(asked.at[:, j], asked.at[:, j], ask_sem.at[2], ask_sem.at[3], "st", z * NJ + (j + t) % NJ).start()
     ek.forward(0)
+    ek.forward(1)
     ev.start(0)
-    ek.forward(1)
-    ev.start(1)
 
     part = wide_w.shape[2] // 2
     half_rows = pl.ds(core * part, part)
@@ -468,10 +473,13 @@
         at = pl.ds(b * 128, 128)
         g[at] = (jax.nn.sigmoid(pv[at].astype(F32)) * g[at].astype(F32)).astype(BF16)
 
+    for ref in (stage.at[0], stage.at[1], stage_k.at[0, 0], stage_k.at[1, 0]):
+        ref[BASE] = jnp.zeros(stage.shape[2:], F32)
     sent_plan.wait()
     ek.first()
     ek.own()
     ek.second()
+    ev.start(1)
     ek.third()
     ev.forward(0)
     ev.forward(1)
@@ -513,6 +521,7 @@
             weight_pass(n, away).start()
     bv.second()
     ev.arrive()
+    bv.third()
 
     @pl.loop(0, blocks)
     def _(b):
@@ -535,7 +544,7 @@
             xk[h, o] = terms[meta[PLACE, o], :, pl.ds(h * HD, HD)]
 
     bk[0].start(-4, 3, -3, 2, -2)
-    bv.third()
+    bv.third_short()
     bk[0].first()
     bk[0].start(1, -1, 0)
     bk[1].start(-4, 3, -3, 2, -2)
@@ -578,6 +587,7 @@
     exchange(2)
     exchange(3)
     bk[0].third()
+    bk[0].third_short()
     bk[1].second()
     for i in range(NZ):
         gwb[i] = dot(rows[:, i * 256 : (i + 1) * 256], pv[...], TN).astype(BF16).reshape(NJ, 32, width)
@@ -590,6 +600,7 @@
         remote(gwb.at[:, other], rs1.at[j], rs_sem.at[0], rs_sem.at[1], "st", z * NJ + other).start()
     bk[0].fourth()
     bk[1].third()
+    bk[1].third_short()
     wait_bytes(rs1.at[pl.ds(0, NJ - 1)], rs_sem.at[1])
     total = gwb[:, j].astype(F32)
     for t in range(1, NJ):
@@ -710,7 +721,8 @@
             pltpu.VMEM((2, 3, PASSAGES) + slim, BF16),
             pltpu.VMEM((blocks, heads, 256, 128), BF16),
             pltpu.VMEM((blocks * 4,) + piece, BF16),
-            pltpu.VMEM((BASE + PASSAGES,) + slim, F32),
+            pltpu.VMEM((2, BASE + 1) + slim, F32),
+            pltpu.VMEM((2, 1, BASE + 1) + slim, F32),
             pltpu.VMEM((rows, width), BF16),
             pltpu.VMEM((2, rows, HD), BF16),
             pltpu.VMEM((2, 2, NST // 2, PLEN, HD * NTP), BF16),
@@ -725,7 +737,7 @@
             dma((2,)),
             dma((2, 1)),
             dma((3, 2)),
-            dma((3, 9)),
+            dma((3, 12)),
             dma((3,)),
             dma((3, NZ)),
             dma((rows // 256,)),

time: 204 us -> 199 us (0.975)
  Pallas kernels: 198 us -> 194 us
    pallas_call x1, Pallas kernels: 198 us -> 194 us  [local(): pl.pallas_call(kernel, out_shape=(jax.ShapeDtypeStruct((tokens, width), B...]
where the time goes in v4:
time: 199 us
  Pallas kernels  194 us (97%)
  other arithmetic  4.22 us (2%)
    pallas_call x1, Pallas kernels, local(): pl.pallas_call(kernel, out_shape=(jax.ShapeDtypeStruct((tokens, width), B...  194 us
    convert_element_type x2, other arithmetic, local(): return (grad_queries.astype(F32), grad_store.astype(F32), grad_w_value)  4.22 us

profile of v4, /device:TPU:1, one launch (start us, length us, event | category | flops | bytes accessed | tf_op | source)
XLA Modules:
  0.0 199.1 jit_solution(17012822271029168321)
XLA Ops:
  0.6 193.6 %passages.1 = (bf16[1024,256]{1,0:T(8,128)(2,1)}, bf16[320,2048]{1,0:T(8,128)(2,1)}, f32[32,256]{1,0:T(8,128)}) custom-call(s32[4,8]{1,0:T(4,128)} %bitcast.8, s32[4,8]{1,0:T(4,128)} %bitcast.9, bf16[1024,256]{1,0:T(8,128)(2,1)} %q_in.1, bf16[1024,256]{1,0:T(8,128)(2,1)} %gate_in.1, bf16[1024,256]{1,0:T(8,128)(2,1)} %cot_in.1, bf16[1280,2048]{1,0:T(8,128)(2,1)} %store_in.1, ...), custom_call_target="tpu_custom_call" | custom-call | flops 10000000000 | bytes 10000000 | tf_op jit(solution)/shard_map/passages/pallas_call | solution.py:686
  194.2 0.0 copy-start
  194.2 0.0 copy-start.1
  194.2 3.2 %convert_element_type.7 = f32[320,2048]{1,0:T(8,128)} convert(bf16[320,2048]{1,0:T(8,128)(2,1)} %get-tuple-element.7) | non-fusion elementwise | flops 655360 | bytes 3932160 | tf_op jit(solution)/shard_map/convert_element_type | solution.py:755
  197.4 0.0 copy-done
  197.4 1.0 convert_element_type.6
  198.5 0.0 copy-done.1
  198.5 0.6 copy.13
Async XLA Ops:
  194.2 3.2 %copy-start = (bf16[1024,256]{1,0:T(8,128)(2,1)S(1)}, bf16[1024,256]{1,0:T(8,128)(2,1)}, u32[]{:S(2)}) copy-start(bf16[1024,256]{1,0:T(8,128)(2,1)} %get-tuple-element.6) | copy-start | bytes 1572868
  194.2 4.2 %copy-start.1 = (f32[32,256]{1,0:T(8,128)S(1)}, f32[32,256]{1,0:T(8,128)}, u32[]{:S(2)}) copy-start(f32[32,256]{1,0:T(8,128)} %get-tuple-element.14) | copy-start | bytes 98308

commit v5 on v4

--- a/solution.py
+++ b/solution.py
@@ -164,6 +164,8 @@
     def third(self):
         self.hop("l4").wait_recv()
         self.hop("l4b").start()
+
+    def third_rest(self):
         self.hop("s3b").wait_recv()
         self.deliver(self.plane(3))
         self.hop("l3").wait_recv()
@@ -423,9 +425,11 @@
             raw = rows[tile].astype(F32)
             rows[tile] = (raw * row_scale(raw) * gain[...]).astype(BF16)
 
-        for n in range(2):
-            weight = x[pl.ds(n * NST // 2, NST // 2)].reshape(rows.shape[1], width)
-            tables[n, pl.ds(4 * i, 4)] = dot(rows[at], weight).astype(BF16).reshape(4, PLEN, width)
+        tabulate(0, i)
+
+    def tabulate(n, i):
+        weight = x[pl.ds(n * NST // 2, NST // 2)].reshape(rows.shape[1], width)
+        tables[n, pl.ds(4 * i, 4)] = dot(rows[chunk(i)], weight).astype(BF16).reshape(4, PLEN, width)
 
     project(0)
     project(1)
@@ -438,6 +442,8 @@
     project(3)
     project(4)
     ek.start(1)
+    for i in range(count):
+        tabulate(1, i)
     wait_bytes(asked.at[pl.ds(0, NZ - 1), 0], ask_sem.at[1])
     for t in range(1, NJ):
         remote(asked.at[:, j], asked.at[:, j], ask_sem.at[2], ask_sem.at[3], "st", z * NJ + (j + t) % NJ).start()
@@ -478,14 +484,15 @@
     sent_plan.wait()
     ek.first()
     ek.own()
+    ev.own()
     ek.second()
+    ek.third()
     ev.start(1)
-    ek.third()
+    ek.third_rest()
     ev.forward(0)
     ev.forward(1)
     ev.first()
     ek.fourth()
-    ev.own()
     ek.arrive()
 
     def joined(n, b, cols):
@@ -512,6 +519,7 @@
 
     bv.start(-4, 3, -3, 2, -2)
     ev.third()
+    ev.third_rest()
     ev.fourth()
     bv.first()
     bv.start(1, -1, 0)

time: 199 us -> 197 us (0.990)
  Pallas kernels: 194 us -> 191 us
    pallas_call x1, Pallas kernels: 194 us -> 191 us  [local(): pl.pallas_call(kernel, out_shape=(jax.ShapeDtypeStruct((tokens, width), B...]
where the time goes in v5:
time: 197 us; the launch traced here: 196 us
  Pallas kernels  191 us (97%)
  other arithmetic  4.22 us (2%)
    pallas_call x1, Pallas kernels, local(): pl.pallas_call(kernel, out_shape=(jax.ShapeDtypeStruct((tokens, width), B...  191 us
    convert_element_type x2, other arithmetic, local(): return (grad_queries.astype(F32), grad_store.astype(F32), grad_w_value)  4.22 us

profile of v5, /device:TPU:1, one launch (start us, length us, event | category | flops | bytes accessed | tf_op | source)
XLA Modules:
  0.0 196.0 jit_solution(11995378247778205925)
XLA Ops:
  0.6 190.5 %passages.1 = (bf16[1024,256]{1,0:T(8,128)(2,1)}, bf16[320,2048]{1,0:T(8,128)(2,1)}, f32[32,256]{1,0:T(8,128)}) custom-call(s32[4,8]{1,0:T(4,128)} %bitcast.8, s32[4,8]{1,0:T(4,128)} %bitcast.9, bf16[1024,256]{1,0:T(8,128)(2,1)} %q_in.1, bf16[1024,256]{1,0:T(8,128)(2,1)} %gate_in.1, bf16[1024,256]{1,0:T(8,128)(2,1)} %cot_in.1, bf16[1280,2048]{1,0:T(8,128)(2,1)} %store_in.1, ...), custom_call_target="tpu_custom_call" | custom-call | flops 10000000000 | bytes 10000000 | tf_op jit(solution)/shard_map/passages/pallas_call | solution.py:694
  191.2 0.0 copy-start
  191.2 0.0 copy-start.1
  191.2 3.2 %convert_element_type.7 = f32[320,2048]{1,0:T(8,128)} convert(bf16[320,2048]{1,0:T(8,128)(2,1)} %get-tuple-element.7) | non-fusion elementwise | flops 655360 | bytes 3932160 | tf_op jit(solution)/shard_map/convert_element_type | solution.py:763
  194.4 0.0 copy-done
  194.4 1.0 convert_element_type.6
  195.4 0.0 copy-done.1
  195.4 0.6 copy.13
Async XLA Ops:
  191.2 3.2 %copy-start = (bf16[1024,256]{1,0:T(8,128)(2,1)S(1)}, bf16[1024,256]{1,0:T(8,128)(2,1)}, u32[]{:S(2)}) copy-start(bf16[1024,256]{1,0:T(8,128)(2,1)} %get-tuple-element.6) | copy-start | bytes 1572868
  191.2 4.2 %copy-start.1 = (f32[32,256]{1,0:T(8,128)S(1)}, f32[32,256]{1,0:T(8,128)}, u32[]{:S(2)}) copy-start(f32[32,256]{1,0:T(8,128)} %get-tuple-element.14) | copy-start | bytes 98308

commit v6 on v5

--- a/solution.py
+++ b/solution.py
@@ -554,9 +554,9 @@
     bk[0].start(-4, 3, -3, 2, -2)
     bv.third_short()
     bk[0].first()
+    bv.fourth()
     bk[0].start(1, -1, 0)
     bk[1].start(-4, 3, -3, 2, -2)
-    bv.fourth()
     bk[0].second()
     bk[1].first()
     bk[1].start(1, -1, 0)

time: 197 us -> 197 us (level)
  no operation moved by 1% of the time
where the time goes in v6:
time: 197 us; the launch traced here: 196 us
  Pallas kernels  191 us (97%)
  other arithmetic  4.22 us (2%)
    pallas_call x1, Pallas kernels, local(): pl.pallas_call(kernel, out_shape=(jax.ShapeDtypeStruct((tokens, width), B...  191 us
    convert_element_type x2, other arithmetic, local(): return (grad_queries.astype(F32), grad_store.astype(F32), grad_w_value)  4.22 us

profile of v6, /device:TPU:1, one launch (start us, length us, event | category | flops | bytes accessed | tf_op | source)
XLA Modules:
  0.0 196.0 jit_solution(6257324424256445961)
XLA Ops:
  0.6 190.5 %passages.1 = (bf16[1024,256]{1,0:T(8,128)(2,1)}, bf16[320,2048]{1,0:T(8,128)(2,1)}, f32[32,256]{1,0:T(8,128)}) custom-call(s32[4,8]{1,0:T(4,128)} %bitcast.8, s32[4,8]{1,0:T(4,128)} %bitcast.9, bf16[1024,256]{1,0:T(8,128)(2,1)} %q_in.1, bf16[1024,256]{1,0:T(8,128)(2,1)} %gate_in.1, bf16[1024,256]{1,0:T(8,128)(2,1)} %cot_in.1, bf16[1280,2048]{1,0:T(8,128)(2,1)} %store_in.1, ...), custom_call_target="tpu_custom_call" | custom-call | flops 10000000000 | bytes 10000000 | tf_op jit(solution)/shard_map/passages/pallas_call | solution.py:694
  191.2 0.0 copy-start
  191.2 0.0 copy-start.1
  191.2 3.2 %convert_element_type.7 = f32[320,2048]{1,0:T(8,128)} convert(bf16[320,2048]{1,0:T(8,128)(2,1)} %get-tuple-element.7) | non-fusion elementwise | flops 655360 | bytes 3932160 | tf_op jit(solution)/shard_map/convert_element_type | solution.py:763
  194.4 0.0 copy-done
  194.4 1.0 convert_element_type.6
  195.4 0.0 copy-done.1
  195.4 0.6 copy.13
Async XLA Ops:
  191.2 3.2 %copy-start = (bf16[1024,256]{1,0:T(8,128)(2,1)S(1)}, bf16[1024,256]{1,0:T(8,128)(2,1)}, u32[]{:S(2)}) copy-start(bf16[1024,256]{1,0:T(8,128)(2,1)} %get-tuple-element.6) | copy-start | bytes 1572868
  191.2 4.2 %copy-start.1 = (f32[32,256]{1,0:T(8,128)S(1)}, f32[32,256]{1,0:T(8,128)}, u32[]{:S(2)}) copy-start(f32[32,256]{1,0:T(8,128)} %get-tuple-element.14) | copy-start | bytes 98308
